TPU v7x, 32 devices: a whole 2x2x4 slice. The times are simulated.
32 devices in a mesh: sp: 8 (over z, core), tp: 4 (over y, x).
Axes of the slice: x: 2, y: 2, z: 4, core: 2. Of those that a mesh axis runs over, the one named last changes fastest.
Arguments:
- tokens: bfloat16 [1536, 4096], P('sp', 'tp'), may hold values from -60 to 60
- lean_query: bfloat16 [1536, 16, 64], P('sp', 'tp'), may hold values from -6 to 6
- lean_key: bfloat16 [1536, 2, 64], P('sp'), may hold values from -6 to 6
- lean_value: bfloat16 [1536, 2, 64], P('sp'), may hold values from -6 to 6
- lean_gains: float32 [2, 64], replicated, may hold values from 0.25 to 7.5
- broad_query: bfloat16 [1536, 16, 128], P('sp', 'tp'), may hold values from -6 to 6
- broad_key: bfloat16 [1536, 2, 128], P('sp'), may hold values from -6 to 6
- broad_value: bfloat16 [1536, 2, 128], P('sp'), may hold values from -6 to 6
- broad_gains: float32 [2, 128], replicated, may hold values from 0.25 to 7.5
- mixer_gain: float32 [3072], replicated, may hold values from 0.1 to 1.9
- output_weight: bfloat16 [3072, 4096], P(None, 'tp'), may hold values from -0.109375 to 0.109375
- channel_gain: float32 [4096], P('tp'), may hold values from 0.1 to 1.9
- gate_weight: bfloat16 [8, 4096, 2048], P('sp', None, 'tp'), may hold values from -0.09375 to 0.09375
- up_weight: bfloat16 [8, 4096, 2048], P('sp', None, 'tp'), may hold values from -0.09375 to 0.09375
- down_weight: bfloat16 [8, 2048, 4096], P('sp', None, 'tp'), may hold values from -0.125 to 0.125
- route_experts: int32 [1536, 2], P('sp'), may hold values from 0 to 7, as said below
- route_logits: float32 [1536, 2], P('sp'), may hold values from -6 to 6
- group_weight: float32 [1536], P('sp'), may hold values from 0.3 to 1
Outputs:
- encoded: bfloat16 [1536, 4096], P('sp', 'tp')
Inputs may be any that keep to these rules, and one draw needn't show every extreme that they name: `route_experts`: each row names two different experts of one group, expert e lying in group e // 2. In every aligned block of 192 rows no expert is named by more than 96 rows; one group, the same for all blocks, is named by exactly half of each block's rows, and each of its experts by exactly 96 of them.
All inputs are finite; a program needn't handle non-finite values.
Results may differ from a plain program's by a relative error of at most 0.0083.
Values may be sent and summed in bfloat16 or wider, within the bound.
A program may use at most 64 MiB of HBM per device.

v0:
```python
import jax
import jax.numpy as jnp
from jax import lax
from jax.sharding import PartitionSpec as P

D = 4096
HQ_A = 16
KV_A = 2
HQ_B = 16
KV_B = 2
GRID_W = 64
GROUPS = 4


epsilon = 1e-06
theta_base = 10000.0
floor_score = -1e30


def axial_angles(positions, head_size):
    quarter = head_size // 4
    frequency = theta_base ** (-jnp.arange(quarter, dtype=jnp.float32) / quarter)
    grid_rows = (positions // GRID_W).astype(jnp.float32)
    grid_columns = (positions % GRID_W).astype(jnp.float32)
    return (grid_rows[:, None] * frequency[None, :], grid_columns[:, None] * frequency[None, :])


def turn_half(values, angles):
    half_width = values.shape[-1] // 2
    first_half = values[..., :half_width]
    second = values[..., half_width:]
    cosine = jnp.cos(angles)[:, None, :]
    sine_part = jnp.sin(angles)[:, None, :]
    return jnp.concatenate(
        [first_half * cosine - second * sine_part, second * cosine + first_half * sine_part],
        axis=-1,
    )


def prepare(raw_values, gain_row, positions):
    values = raw_values.astype(jnp.float32)
    values = (
        values * lax.rsqrt(jnp.mean(values * values, axis=-1, keepdims=True) + epsilon) * gain_row
    )
    row_angles, column_angles = axial_angles(positions, raw_values.shape[-1])
    half_width = raw_values.shape[-1] // 2
    turned = jnp.concatenate(
        [
            turn_half(values[..., :half_width], row_angles),
            turn_half(values[..., half_width:], column_angles),
        ],
        axis=-1,
    )
    return turned.astype(jnp.bfloat16)


def group_norm(head_rows, gain_row):
    values = head_rows.astype(jnp.float32)
    return (
        values * lax.rsqrt(jnp.mean(values * values, axis=-1, keepdims=True) + epsilon) * gain_row
    ).astype(jnp.bfloat16)


def own_heads(query_raw, key_raw, value_raw, gain_pair, positions, lane_index, group_ratio):
    head_count, head_size = (query_raw.shape[1], query_raw.shape[2])
    key_heads = max(1, head_count // group_ratio)
    kv_start = lane_index * head_count // group_ratio
    key_part = lax.dynamic_slice_in_dim(key_raw, kv_start, key_heads, 1)
    value_part = lax.dynamic_slice_in_dim(value_raw, kv_start, key_heads, 1)
    queries = prepare(query_raw, gain_pair[0], positions).reshape(
        query_raw.shape[0], key_heads, head_count // key_heads, head_size
    )
    return (queries, prepare(key_part, gain_pair[1], positions), value_part)


def start_state(queries):
    row_count = queries.shape[0]
    head_count = queries.shape[1] * queries.shape[2]
    return (
        jnp.full((head_count, row_count), floor_score, jnp.float32),
        jnp.zeros((head_count, row_count), jnp.float32),
        jnp.zeros((row_count, head_count, queries.shape[3]), jnp.float32),
    )


def attend_piece(fold_state, queries, keys, values):
    peak_score, weight_sum, accumulated = fold_state
    row_count, key_heads, grouped, head_size = queries.shape
    key_count = keys.shape[0]
    scores = jnp.einsum(
        "qkgd,skd->kgqs", queries, keys, preferred_element_type=jnp.float32
    ) * head_size ** (-0.5)
    scores = scores.reshape(key_heads * grouped, row_count, key_count)
    new_peak = jnp.maximum(peak_score, jnp.max(scores, axis=-1))
    weights = jnp.exp(scores - new_peak[..., None])
    new_sum = jnp.sum(weights, axis=-1)
    rounded = weights.astype(jnp.bfloat16).reshape(key_heads, grouped, row_count, key_count)
    partial_value = jnp.einsum(
        "kgqs,skd->qkgd", rounded, values, preferred_element_type=jnp.float32
    )
    partial_value = partial_value.reshape(row_count, key_heads * grouped, head_size)
    return (new_peak, new_sum, partial_value)


def finish_heads(fold_state):
    accumulated = fold_state[2]
    return (
        (accumulated / jnp.transpose(fold_state[1])[:, :, None])
        .astype(jnp.bfloat16)
        .reshape(accumulated.shape[0], -1)
    )


def on_device(
    tokens,
    lean_query,
    lean_key,
    lean_value,
    lean_gains,
    broad_query,
    broad_key,
    broad_value,
    broad_gains,
    mixer_gain,
    output_weight,
    channel_gain,
    gate_weight,
    up_weight,
    down_weight,
    route_experts,
    route_logits,
    group_weight,
):
    row_count = tokens.shape[0]
    positions = lax.axis_index("sp") * row_count + jnp.arange(row_count, dtype=jnp.int32)
    lane_index = lax.axis_index("tp")
    lean_queries, lean_keys, lean_values = own_heads(
        lean_query, lean_key, lean_value, lean_gains, positions, lane_index, HQ_A // KV_A
    )
    broad_queries, broad_keys, broad_values = own_heads(
        broad_query, broad_key, broad_value, broad_gains, positions, lane_index, HQ_B // KV_B
    )
    shard_rows = (
        lax.all_gather(lean_keys, "sp", axis=0, tiled=True),
        lax.all_gather(lean_values, "sp", axis=0, tiled=True),
        lax.all_gather(broad_keys, "sp", axis=0, tiled=True),
        lax.all_gather(broad_values, "sp", axis=0, tiled=True),
    )
    lean_state = attend_piece(start_state(lean_queries), lean_queries, shard_rows[0], shard_rows[1])
    broad_state = attend_piece(
        start_state(broad_queries), broad_queries, shard_rows[2], shard_rows[3]
    )
    lean_all, broad_all = (
        lax.all_gather(finish_heads(lean_state), "tp", axis=1, tiled=True),
        lax.all_gather(finish_heads(broad_state), "tp", axis=1, tiled=True),
    )
    lean_width = lean_all.shape[1]
    stream = tokens.astype(jnp.float32) + jnp.dot(
        group_norm(lean_all, mixer_gain[:lean_width]),
        output_weight[:lean_width],
        preferred_element_type=jnp.float32,
    )
    stream = stream + jnp.dot(
        group_norm(broad_all, mixer_gain[lean_width:]),
        output_weight[lean_width:],
        preferred_element_type=jnp.float32,
    )
    squares = lax.psum(jnp.sum(stream * stream, axis=1), "tp")
    normed = (stream * lax.rsqrt(squares / D + epsilon)[:, None] * channel_gain).astype(
        jnp.bfloat16
    )
    experts = lax.axis_size("sp")
    capacity = row_count // (experts // GROUPS)
    flat_experts = route_experts.reshape(-1)
    onehot = (flat_experts[:, None] == jnp.arange(experts, dtype=jnp.int32)[None, :]).astype(
        jnp.int32
    )
    slot_rank = jnp.sum((jnp.cumsum(onehot, axis=0) - 1) * onehot, axis=1)
    slot_index = flat_experts * capacity + slot_rank
    token_owner = jnp.repeat(jnp.arange(row_count, dtype=jnp.int32), route_experts.shape[1])
    filled = jnp.zeros((experts * capacity,), jnp.int32).at[slot_index].set(token_owner + 1)
    slot_live = (filled > 0)[:, None]
    source = jnp.maximum(filled - 1, 0)
    outgoing = jnp.where(slot_live, normed[source], jnp.zeros((), jnp.bfloat16)).reshape(
        experts, capacity, -1
    )
    arrived = lax.all_to_all(outgoing, "sp", split_axis=0, concat_axis=0, tiled=True)
    sources = arrived.shape[0]
    item_count = arrived.shape[1]
    shard_rows = lax.all_gather(arrived, "tp", axis=2, tiled=True)
    flat_rows = shard_rows.reshape(sources * item_count, shard_rows.shape[2])
    gate_part = gate_weight[0]
    up_part = up_weight[0]
    gate_value = jnp.dot(flat_rows, gate_part, preferred_element_type=jnp.float32)
    up_value = jnp.dot(flat_rows, up_part, preferred_element_type=jnp.float32)
    hidden = (jax.nn.silu(gate_value) * up_value).astype(jnp.bfloat16)
    down_part = down_weight[0]
    result = jnp.dot(
        lax.all_gather(hidden, "tp", axis=1, tiled=True),
        down_part,
        preferred_element_type=jnp.float32,
    )
    result = result.astype(jnp.bfloat16).reshape(sources, item_count, -1)
    returned = lax.all_to_all(result, "sp", split_axis=0, concat_axis=0, tiled=True)
    picked = (
        returned.reshape(experts * capacity, -1)[slot_index]
        .reshape(row_count, route_experts.shape[1], -1)
        .astype(jnp.float32)
    )
    logit_gap = route_logits[:, 0] - route_logits[:, 1]
    weights = group_weight[:, None] * jax.nn.sigmoid(jnp.stack([logit_gap, -logit_gap], axis=1))
    return (stream + jnp.sum(picked * weights[:, :, None], axis=1)).astype(jnp.bfloat16)


def solution(mesh):
    return jax.shard_map(
        on_device,
        mesh=mesh,
        in_specs=(
            P("sp", "tp"),
            P("sp", "tp", None),
            P("sp", None, None),
            P("sp", None, None),
            P(),
            P("sp", "tp", None),
            P("sp", None, None),
            P("sp", None, None),
            P(),
            P(),
            P(None, "tp"),
            P("tp"),
            P("sp", None, "tp"),
            P("sp", None, "tp"),
            P("sp", None, "tp"),
            P("sp", None),
            P("sp", None),
            P("sp"),
        ),
        out_specs=P("sp", "tp"),
        check_vma=False,
    )
```

profile of v0, /device:TPU:0, one launch (start us, length us, event | category | flops | bytes accessed | tf_op | source)
XLA Modules:
  0.0 365.0 jit_solution(18424570227048056855)
XLA Ops:
  10.1 2.9 scatter_custom_fusion
  16.0 17.2 %all_gather.25 = bf16[1536,1,64]{2,1,0:T(2,128)(2,1)S(1)} all-gather(bf16[192,1,64]{2,1,0:T(2,128)(2,1)S(1)} %copy.73), channel_id=1, replica_groups=mesh['sp'=8,'tp'=4] {'sp'}, dimensions={0}, use_global_device_ids=true | all-gather | bytes 221184 | tf_op jit(solution)/shard_map/all_gather | solution.py:144
  35.7 2.9 bitcast_reduce_fusion.1
  38.8 15.7 %all_gather.24 = bf16[1536,1,64]{2,1,0:T(2,128)(2,1)S(1)} all-gather(bf16[192,1,64]{2,1,0:T(2,128)(2,1)S(1)} %copy.85), channel_id=1, replica_groups=mesh['sp'=8,'tp'=4] {'sp'}, dimensions={0}, use_global_device_ids=true | all-gather | bytes 221184 | tf_op jit(solution)/shard_map/all_gather | solution.py:145
  55.0 3.4 fusion.3
  58.8 1.0 fusion.22
  59.8 10.3 %all_gather.26 = bf16[192,1024]{0,1:T(8,128)(2,1)S(1)} all-gather(bf16[192,256]{0,1:T(8,128)(2,1)S(1)} %fusion.60), channel_id=1, replica_groups=mesh['sp'=8,'tp'=4] {'tp'}, dimensions={1}, use_global_device_ids=true | all-gather | bytes 491520 | tf_op jit(solution)/shard_map/all_gather | solution.py:154
  72.0 15.2 %all_gather.28 = bf16[1536,1,128]{2,0,1:T(8,128)(2,1)S(1)} all-gather(bf16[192,1,128]{2,0,1:T(8,128)(2,1)S(1)} %copy.77), channel_id=1, replica_groups=mesh['sp'=8,'tp'=4] {'sp'}, dimensions={0}, use_global_device_ids=true | all-gather | bytes 442368 | tf_op jit(solution)/shard_map/all_gather | solution.py:146
  89.1 14.6 %all_gather.27 = bf16[1536,1,128]{2,0,1:T(8,128)(2,1)S(1)} all-gather(bf16[192,1,128]{2,0,1:T(8,128)(2,1)S(1)} %copy.86), channel_id=1, replica_groups=mesh['sp'=8,'tp'=4] {'sp'}, dimensions={0}, use_global_device_ids=true | all-gather | bytes 442368 | tf_op jit(solution)/shard_map/all_gather | solution.py:147
  106.3 12.5 %all_gather.29 = bf16[192,2048]{1,0:T(8,128)(2,1)S(1)} all-gather(bf16[192,512]{1,0:T(8,128)(2,1)S(1)} %fusion.54), channel_id=1, replica_groups=mesh['sp'=8,'tp'=4] {'tp'}, dimensions={1}, use_global_device_ids=true | all-gather | bytes 983040 | tf_op jit(solution)/shard_map/all_gather | solution.py:155
  119.0 3.3 fusion.14
  122.3 2.6 multiply_reduce_fusion.1
  124.9 8.9 %psum.7 = f32[192]{0:T(256)S(1)} all-reduce(f32[192]{0:T(256)S(1)} %get-tuple-element.51), channel_id=1, replica_groups=mesh['sp'=8,'tp'=4] {'tp'}, use_global_device_ids=true, to_apply=%region_15.16 | all-reduce | flops 192 | bytes 1536 | tf_op jit(solution)/shard_map/psum | solution.py:168
  134.1 2.8 gather_fusion
  137.1 42.5 %all_to_all.10 = bf16[8,96,1024]{2,1,0:T(8,128)(2,1)} all-to-all(bf16[8,96,1024]{2,1,0:T(8,128)(2,1)S(1)} %broadcast_select_fusion), channel_id=1, replica_groups=mesh['sp'=8,'tp'=4] {'sp'}, dimensions={0} | all-to-all | bytes 3145728 | tf_op jit(solution)/shard_map/all_to_all | solution.py:187
  179.7 67.2 %all-gather.3.cloned.1.call-done = bf16[8,96,4096]{2,1,0:T(8,128)(2,1)} async-done(((bf16[8,96,1024]{2,1,0:T(8,128)(2,1)}), bf16[8,96,4096]{2,1,0:T(8,128)(2,1)}) %all-gather.3.cloned.1.call-update) | async-done | bytes 6291472 | tf_op jit(solution)/shard_map/all_gather | solution.py:190
  246.8 6.9 %fusion.12 = f32[768,512]{1,0:T(8,128)S(1)} fusion(bf16[768,4096]{1,0:T(8,128)(2,1)} %bitcast.137, bf16[1,4096,512]{2,1,0:T(8,128)(2,1)} %param.30), kind=kOutput, calls=%fused_computation.21 | convolution fusion | flops 3221225472 | bytes 12058624 | tf_op jit(solution)/shard_map/dot_general | solution.py:194
  253.9 4.4 %multiply_convert_fusion = bf16[768,512]{1,0:T(8,128)(2,1)} fusion(f32[768,512]{1,0:T(8,128)S(1)} %fusion.12, bf16[768,4096]{1,0:T(8,128)(2,1)S(1)} %bitcast.138, bf16[1,4096,512]{2,1,0:T(8,128)(2,1)S(1)} %copy-done.10), kind=kOutput, calls=%fused_computation.40 | convolution fusion | flops 3223584768 | bytes 12845056 | tf_op jit(solution)/shard_map/dot_general | solution.py:195
  258.4 43.8 %all-gather.5.cloned.1.call-done = bf16[768,2048]{1,0:T(8,128)(2,1)} async-done(((bf16[768,512]{1,0:T(8,128)(2,1)}), bf16[768,2048]{1,0:T(8,128)(2,1)}) %all-gather.5.cloned.1.call-update) | async-done | bytes 3145744 | tf_op jit(solution)/shard_map/all_gather | solution.py:199
  302.2 7.7 %fusion.26 = bf16[768,1024]{1,0:T(8,128)(2,1)} fusion(bf16[768,2048]{1,0:T(8,128)(2,1)} %all-gather.5.cloned.1.call-done, bf16[1,2048,1024]{2,1,0:T(8,128)(2,1)} %param.32), kind=kOutput, calls=%fused_computation.35 | convolution fusion | flops 3222011904 | bytes 8912896 | tf_op jit(solution)/shard_map/dot_general | solution.py:198
  309.9 4.6 %all-to-all-start.1 = ((bf16[8,96,1024]{2,1,0:T(8,128)(2,1)}), bf16[8,96,1024]{2,1,0:T(8,128)(2,1)S(1)}, u32[]{:S(2)}, u32[]{:S(2)}) async-start(bf16[8,96,1024]{2,1,0:T(8,128)(2,1)} %bitcast.131), calls=%async_computation.1 | async-start | bytes 3145728 | tf_op jit(solution)/shard_map/all_to_all | solution.py:204
  314.7 37.6 %all-to-all-done.1 = bf16[8,96,1024]{2,1,0:T(8,128)(2,1)S(1)} async-done(((bf16[8,96,1024]{2,1,0:T(8,128)(2,1)}), bf16[8,96,1024]{2,1,0:T(8,128)(2,1)S(1)}, u32[]{:S(2)}, u32[]{:S(2)}) %all-to-all-start.1) | async-done | bytes 1572896 | tf_op jit(solution)/shard_map/all_to_all | solution.py:204
  352.3 2.1 gather_fusion.1
  355.4 2.0 multiply_reduce_fusion
  (108 shorter events, 18.9 us)
Async XLA Ops:
  6.5 63.8 %copy-start = (bf16[192,2,128]{2,1,0:T(2,128)(2,1)S(1)}, bf16[192,2,128]{2,1,0:T(2,128)(2,1)}, u32[]{:S(2)}) copy-start(bf16[192,2,128]{2,1,0:T(2,128)(2,1)} %param.24) | copy-start | bytes 294916
  6.5 240.3 %all-gather.3.cloned.1.call-start = ((), (), s32[]{:S(2)}) async-start(), calls=%async_computation.2 | async-start | bytes 7864320 | tf_op jit(solution)/shard_map/all_gather | solution.py:190
  14.6 24.1 %copy-start.4 = (bf16[192,2,64]{0,2,1:T(8,128)(2,1)S(1)}, bf16[192,2,64]{0,2,1:T(8,128)(2,1)}, u32[]{:S(2)}) copy-start(bf16[192,2,64]{0,2,1:T(8,128)(2,1)} %param.21) | copy-start | bytes 147460
  55.0 3.8 %copy-start.1 = (f32[1536,192,4]{0,1,2:T(8,128)S(1)}, f32[1536,192,4]{0,1,2:T(8,128)}, u32[]{:S(2)}) copy-start(f32[1536,192,4]{0,1,2:T(8,128)} %get-tuple-element.50) | copy-start | bytes 14155780
  58.8 11.9 %copy-start.8 = (f32[2,128]{1,0:T(2,128)S(1)}, f32[2,128]{1,0:T(2,128)}, u32[]{:S(2)}) copy-start(f32[2,128]{1,0:T(2,128)} %param.26) | copy-start | bytes 3076
  58.8 28.4 %copy-start.2 = (bf16[192,4,128]{2,1,0:T(4,128)(2,1)S(1)}, bf16[192,4,128]{2,1,0:T(4,128)(2,1)}, u32[]{:S(2)}) copy-start(bf16[192,4,128]{2,1,0:T(4,128)(2,1)} %param.23) | copy-start | bytes 589828
  87.6 1.4 copy-start.3
  104.6 14.4 %slice-start = ((f32[3072]{0:T(1024)}), f32[2048]{0:T(1024)S(1)}, s32[]{:S(2)}) async-start(f32[3072]{0:T(1024)} %param.27), calls=%async_computation.4 | async-start | bytes 16384 | tf_op jit(solution)/shard_map/slice | solution.py:164
  119.0 3.3 slice-start.1
  119.0 3.3 copy-start.11
  122.3 11.6 %copy-start.5 = (f32[1024]{0:T(1024)S(1)}, f32[1024]{0:T(1024)}, u32[]{:S(2)}) copy-start(f32[1024]{0:T(1024)} %param.29) | copy-start | bytes 12292
  179.6 122.6 %all-gather.5.cloned.1.call-start = ((), (), s32[]{:S(2)}) async-start(), calls=%async_computation.3 | async-start | bytes 3932160 | tf_op jit(solution)/shard_map/all_gather | solution.py:199
  246.8 6.9 %copy-start.9 = (bf16[8,96,4096]{2,1,0:T(8,128)(2,1)S(1)}, bf16[8,96,4096]{2,1,0:T(8,128)(2,1)}, u32[]{:S(2)}) copy-start(bf16[8,96,4096]{2,1,0:T(8,128)(2,1)} %all-gather.3.cloned.1.call-done) | copy-start | bytes 18874372
  246.8 7.0 %copy-start.10 = (bf16[1,4096,512]{2,1,0:T(8,128)(2,1)S(1)}, bf16[1,4096,512]{2,1,0:T(8,128)(2,1)}, u32[]{:S(2)}) copy-start(bf16[1,4096,512]{2,1,0:T(8,128)(2,1)} %param.31) | copy-start | bytes 12582916
  258.3 56.2 %copy-start.6 = (f32[192,2]{0,1:T(2,128)S(1)}, f32[192,2]{0,1:T(2,128)}, u32[]{:S(2)}) copy-start(f32[192,2]{0,1:T(2,128)} %param.34) | copy-start | bytes 4612
  258.4 56.2 %copy-start.7 = (f32[192]{0:T(256)S(1)}, f32[192]{0:T(256)}, u32[]{:S(2)}) copy-start(f32[192]{0:T(256)} %param.35) | copy-start | bytes 2308
  309.9 42.4 %all-to-all-start.1 = ((bf16[8,96,1024]{2,1,0:T(8,128)(2,1)}), bf16[8,96,1024]{2,1,0:T(8,128)(2,1)S(1)}, u32[]{:S(2)}, u32[]{:S(2)}) async-start(bf16[8,96,1024]{2,1,0:T(8,128)(2,1)} %bitcast.131), calls=%async_computation.1 | async-start | bytes 3145728 | tf_op jit(solution)/shard_map/all_to_all | solution.py:204
Sparse Core Ops, SparseCore 0:
  179.7 67.0 all-gather.2
  258.5 43.7 all-gather.4
where the time goes:
time: 366 us; the launch traced here: 365 us
  waiting for transfers between devices  149 us (41%)
  blocking collectives  137 us (37%)
  matrix products  30.7 us (8%)
  other arithmetic  15.9 us (4%)
  local copies, waits for them, and re-layouts  14.3 us (4%)
  between operations  13.9 us (4%)
  starting transfers between devices  4.65 us (1%)
    all_gather x1, waiting for transfers between devices, on_device(): shard_rows = lax.all_gather(arrived, 'tp', axis=2, tiled=True)  67.2 us
    all_gather x1, waiting for transfers between devices, on_device(): lax.all_gather(hidden, 'tp', axis=1, tiled=True)  43.8 us
    all_to_all x1, blocking collectives, on_device(): lax.all_to_all(outgoing, 'sp', split_axis=0, concat_axis=0, tiled=True)  42.5 us
    all_to_all x1, waiting for transfers between devices, on_device(): lax.all_to_all(result, 'sp', split_axis=0, concat_axis=0, tiled=True)  37.6 us
    all_gather x1, blocking collectives, on_device(): lax.all_gather(lean_keys, 'sp', axis=0, tiled=True)  17.2 us
    all_gather x1, blocking collectives, on_device(): lax.all_gather(lean_values, 'sp', axis=0, tiled=True)  15.7 us
    all_gather x1, blocking collectives, on_device(): lax.all_gather(broad_keys, 'sp', axis=0, tiled=True)  15.2 us
    all_gather x1, blocking collectives, on_device(): lax.all_gather(broad_values, 'sp', axis=0, tiled=True)  14.6 us
  transfers between devices with their start and end apart: 3, of which 3 were waited for; matrix products, arithmetic and copies ran while one was open for 0% of the time, Pallas kernels for 0%

commit v1 on v0

--- a/solution.py
+++ b/solution.py
@@ -1,6 +1,10 @@
+import functools
+
 import jax
 import jax.numpy as jnp
 from jax import lax
+from jax.experimental import pallas as pl
+from jax.experimental.pallas import tpu as pltpu
 from jax.sharding import PartitionSpec as P
 
 D = 4096
@@ -109,6 +113,393 @@
         .astype(jnp.bfloat16)
         .reshape(accumulated.shape[0], -1)
     )
+
+
+MESH = pl.DeviceIdType.MESH
+EXTRA = 128
+
+
+def enter(peers):
+    barrier = pltpu.get_barrier_semaphore()
+    for peer in peers:
+        pl.semaphore_signal(barrier, inc=1, device_id=peer, device_id_type=MESH)
+    pl.semaphore_wait(barrier, len(peers))
+
+
+def place():
+    sp, tp = lax.axis_index("sp"), lax.axis_index("tp")
+    z, core = sp // 2, sp % 2
+    y, x = tp // 2, tp % 2
+    sibling = {"sp": z * 2 + (1 - core), "tp": tp}
+    x_peer = {"sp": sp, "tp": y * 2 + (1 - x)}
+    y_peer = {"sp": sp, "tp": (1 - y) * 2 + x}
+    chunks = (tp, y * 2 + (1 - x), (1 - y) * 2 + x, (1 - y) * 2 + (1 - x))
+    return z, core, tp, sibling, x_peer, y_peer, chunks
+
+
+def remote(source, target, send_sem, recv_sem, device):
+    return pltpu.make_async_remote_copy(
+        src_ref=source,
+        dst_ref=target,
+        send_sem=send_sem,
+        recv_sem=recv_sem,
+        device_id=device,
+        device_id_type=MESH,
+    )
+
+
+def keys_kernel(chips, own_ref, out_ref, z_send, z_recv, s_send, s_recv):
+    z, core, tp, sibling, x_peer, y_peer, chunks = place()
+    peers = [{"sp": ((z + d) % chips) * 2 + core, "tp": tp} for d in range(1, chips)]
+    enter(peers + [sibling])
+    sends = [
+        remote(own_ref, out_ref.at[0, d], z_send.at[d], z_recv.at[d], peers[d - 1])
+        for d in range(1, chips)
+    ]
+    for copy in sends:
+        copy.start()
+    forwards = [remote(own_ref, out_ref.at[1, 0], s_send.at[0], s_recv.at[0], sibling)]
+    forwards[0].start()
+    out_ref[0, 0] = own_ref[...]
+    for d in range(1, chips):
+        sends[d - 1].wait_recv()
+        copy = remote(out_ref.at[0, d], out_ref.at[1, d], s_send.at[d], s_recv.at[d], sibling)
+        copy.start()
+        forwards.append(copy)
+    for copy in forwards:
+        copy.wait()
+    for copy in sends:
+        copy.wait_send()
+
+
+def gather_keys(own, chips):
+    return pl.pallas_call(
+        functools.partial(keys_kernel, chips),
+        out_shape=jax.ShapeDtypeStruct((2, chips) + own.shape, own.dtype),
+        in_specs=[pl.BlockSpec(memory_space=pltpu.VMEM)],
+        out_specs=pl.BlockSpec(memory_space=pltpu.VMEM),
+        scratch_shapes=[pltpu.SemaphoreType.DMA((chips,))] * 4,
+        compiler_params=pltpu.CompilerParams(collective_id=0, has_side_effects=True),
+    )(own)
+
+
+def heads_kernel(lean_ref, broad_ref, lean_out, broad_out, send_sem, recv_sem):
+    z, core, tp, sibling, x_peer, y_peer, chunks = place()
+    enter([x_peer, y_peer])
+    half = lean_ref.shape[0] // 2
+    pieces = ((lean_ref, lean_out), (broad_ref, broad_out))
+
+    def columns(ref, chunk):
+        width = ref.shape[1]
+        return pl.ds(pl.multiple_of(chunk * width, width), width)
+
+    first = []
+    for i, (own, out) in enumerate(pieces):
+        for j, peer in enumerate((x_peer, y_peer)):
+            k = i * 2 + j
+            copy = remote(own, out.at[:, columns(own, tp)], send_sem.at[k], recv_sem.at[k], peer)
+            copy.start()
+            first.append(copy)
+    for own, out in pieces:
+        out[:, columns(own, tp)] = own[...]
+    second = []
+    for i, (own, out) in enumerate(pieces):
+        for j, peer in enumerate((y_peer, x_peer)):
+            first[i * 2 + j].wait_recv()
+            k = 4 + i * 2 + j
+            part = out.at[pl.ds(j * half, half), columns(own, chunks[1 + j])]
+            copy = remote(part, part, send_sem.at[k], recv_sem.at[k], peer)
+            copy.start()
+            second.append(copy)
+    for copy in second:
+        copy.wait()
+    for copy in first:
+        copy.wait_send()
+
+
+def gather_heads(lean, broad, lanes):
+    return pl.pallas_call(
+        heads_kernel,
+        out_shape=[
+            jax.ShapeDtypeStruct((part.shape[0], part.shape[1] * lanes), part.dtype)
+            for part in (lean, broad)
+        ],
+        in_specs=[pl.BlockSpec(memory_space=pltpu.VMEM)] * 2,
+        out_specs=[pl.BlockSpec(memory_space=pltpu.VMEM)] * 2,
+        scratch_shapes=[pltpu.SemaphoreType.DMA((8,))] * 2,
+        compiler_params=pltpu.CompilerParams(collective_id=1, has_side_effects=True),
+    )(lean, broad)
+
+
+def experts_kernel(
+    width,
+    out_going,
+    gate_hbm,
+    up_hbm,
+    down_hbm,
+    out_ref,
+    rows,
+    gate_w,
+    up_w,
+    down_w,
+    hidden,
+    gate_acc,
+    up_acc,
+    result,
+    swap_send,
+    swap_recv,
+    back,
+    w_sem,
+    send_sem,
+    recv_sem,
+    h_send,
+    h_recv,
+    e_send,
+    e_recv,
+    b_send,
+    b_recv,
+):
+    z, core, tp, sibling, x_peer, y_peer, chunks = place()
+    chips, cap = out_going.shape[0], out_going.shape[1]
+    ff = gate_acc.shape[1]
+    half = 2 * cap
+    ahead = [{"sp": ((z + d) % chips) * 2 + core, "tp": tp} for d in range(chips)]
+    behind = [{"sp": ((z + chips - d) % chips) * 2 + core, "tp": tp} for d in range(chips)]
+    enter(ahead[1:] + [sibling, x_peer, y_peer])
+
+    def slot(d, r, side=0):
+        return rows.at[d // 2, r, pl.ds(side * half + (d % 2) * cap, cap)]
+
+    Z, X, Y, RELAY, SIDE = 0, 1, 2, 3, 4
+    pending = []
+
+    def send(source, target, kind, d, device):
+        copy = remote(source, target, send_sem.at[kind, d], recv_sem.at[kind, d], device)
+        copy.start()
+        pending.append(copy)
+        return copy
+
+    arrivals = {}
+    for d in range(1, chips):
+        arrivals[Z, d] = send(out_going.at[d], slot(d, 0), Z, d, ahead[d])
+    loads = [
+        pltpu.make_async_copy(source, target, w_sem.at[i])
+        for i, (source, target) in enumerate(
+            ((gate_hbm, gate_w), (up_hbm, up_w), (down_hbm, down_w))
+        )
+    ]
+
+    def spread(d):
+        source = out_going.at[0] if d == 0 else slot(d, 0)
+        if d:
+            arrivals[Z, d].wait_recv()
+        arrivals[X, d] = send(source, slot(d, 1), X, d, x_peer)
+        arrivals[Y, d] = send(source, slot(d, 2), Y, d, y_peer)
+        arrivals[SIDE, d] = send(source, slot(d, 0, 1), SIDE, d, sibling)
+
+    def to_side(d, r):
+        arrivals[SIDE + r, d] = send(slot(d, r), slot(d, r, 1), SIDE + r, d, sibling)
+
+    def relay(d):
+        arrivals[X, d].wait_recv()
+        if d % 2 == 0:
+            arrivals[RELAY, d] = send(slot(d, 1), slot(d, 3), RELAY, d, y_peer)
+        to_side(d, 1)
+        arrivals[Y, d].wait_recv()
+        if d % 2 == 1:
+            arrivals[RELAY, d] = send(slot(d, 2), slot(d, 3), RELAY, d, x_peer)
+        to_side(d, 2)
+
+    def project(p, r):
+        for d in (2 * p, 2 * p + 1):
+            arrivals[SIDE + r, d].wait_recv()
+        block = rows[p, r, :, pl.ds(0, width)]
+        for weight, total in ((gate_w, gate_acc), (up_w, up_acc)):
+            part = jnp.dot(block, weight[chunks[r]], preferred_element_type=jnp.float32)
+            if r == 0:
+                total[...] = part
+            else:
+                total[...] += part
+
+    def activate(p):
+        squares = 0.0
+        for r in range(4):
+            extra = rows[p, r, :, pl.ds(width, EXTRA)].astype(jnp.float32)
+            squares = squares + extra[:, 0:1] + extra[:, 1:2]
+        scale = lax.rsqrt(squares / (4 * width) + epsilon)
+        gate_value = gate_acc[...] * scale
+        up_value = up_acc[...] * scale
+        hidden[p, 0] = (gate_value / (1.0 + jnp.exp(-gate_value)) * up_value).astype(jnp.bfloat16)
+        for k, peer in ((0, x_peer), (1, y_peer)):
+            copy = remote(
+                hidden.at[p, 0], hidden.at[p, 1 + k], h_send.at[p, k], h_recv.at[p, k], peer
+            )
+            copy.start()
+            pending.append(copy)
+            arrivals["h", p, k] = copy
+
+    def relay_hidden(p):
+        for k, peer in ((0, y_peer), (1, x_peer)):
+            arrivals["h", p, k].wait_recv()
+            part = pl.ds(k * half, half)
+            copy = remote(
+                hidden.at[p, 1 + k, part],
+                hidden.at[p, 3, part],
+                h_send.at[p, 2 + k],
+                h_recv.at[p, 2 + k],
+                peer,
+            )
+            copy.start()
+            pending.append(copy)
+            arrivals["h", p, 2 + k] = copy
+
+    def last_slot(p):
+        for d in (2 * p, 2 * p + 1):
+            arrivals[RELAY, d].wait_recv()
+            to_side(d, 3)
+        project(p, 3)
+        activate(p)
+
+    def finish(p):
+        for r in range(3):
+            part = jnp.dot(hidden[p, r], down_w[chunks[r]], preferred_element_type=jnp.float32)
+            if r == 0:
+                result[...] = part
+            else:
+                result[...] += part
+        for k in (2, 3):
+            arrivals["h", p, k].wait_recv()
+        result[...] += jnp.dot(hidden[p, 3], down_w[chunks[3]], preferred_element_type=jnp.float32)
+        extra = rows[p, 0, :, pl.ds(width, EXTRA)].astype(jnp.float32)
+        low = extra[:, 2:3] + extra[:, 3:4]
+        high = extra[:, 4:5] + extra[:, 5:6]
+        share = low + (high - low) * core.astype(jnp.float32)
+        swap_send[p] = (result[half:, :] * share[half:]).astype(jnp.bfloat16)
+        copy = remote(swap_send.at[p], swap_recv.at[p], e_send.at[p], e_recv.at[p], sibling)
+        copy.start()
+        pending.append(copy)
+        kept = result[:half, :] * share[:half]
+        copy.wait_recv()
+        total = (kept + swap_recv[p].astype(jnp.float32)).astype(jnp.bfloat16)
+        back[p] = total
+        for d in (2 * p, 2 * p + 1):
+            part = pl.ds((d % 2) * cap, cap)
+            if d == 0:
+                out_ref[0] = total[:cap]
+                continue
+            copy = remote(back.at[p, part], out_ref.at[d], b_send.at[d], b_recv.at[d], behind[d])
+            copy.start()
+            pending.append(copy)
+            arrivals["b", d] = copy
+
+    spread(0)
+    for copy in loads:
+        copy.start()
+    rows[0, 0, pl.ds(0, cap)] = out_going[0]
+    spread(1)
+    relay(0)
+    relay(1)
+    spread(2)
+    spread(3)
+    loads[0].wait()
+    loads[1].wait()
+    for r in range(3):
+        project(0, r)
+    last_slot(0)
+    relay(2)
+    relay(3)
+    relay_hidden(0)
+    for r in range(3):
+        project(1, r)
+    last_slot(1)
+    loads[2].wait()
+    finish(0)
+    relay_hidden(1)
+    finish(1)
+    for d in range(1, chips):
+        arrivals["b", d].wait_recv()
+    for copy in pending:
+        copy.wait_send()
+
+
+def run_experts(out_going, gate_weight, up_weight, down_weight):
+    chips, cap, padded = out_going.shape
+    width, ff = (padded - EXTRA, gate_weight.shape[1])
+    features = down_weight.shape[1]
+    return pl.pallas_call(
+        functools.partial(experts_kernel, width),
+        out_shape=jax.ShapeDtypeStruct((chips, cap, features), jnp.bfloat16),
+        in_specs=[pl.BlockSpec(memory_space=pltpu.VMEM)]
+        + [pl.BlockSpec(memory_space=pl.ANY)] * 3,
+        out_specs=pl.BlockSpec(memory_space=pltpu.VMEM),
+        scratch_shapes=[
+            pltpu.VMEM((2, 4, 4 * cap, padded), jnp.bfloat16),
+            pltpu.VMEM((4, width, ff), jnp.bfloat16),
+            pltpu.VMEM((4, width, ff), jnp.bfloat16),
+            pltpu.VMEM((4, ff, features), jnp.bfloat16),
+            pltpu.VMEM((2, 4, 4 * cap, ff), jnp.bfloat16),
+            pltpu.VMEM((4 * cap, ff), jnp.float32),
+            pltpu.VMEM((4 * cap, ff), jnp.float32),
+            pltpu.VMEM((4 * cap, features), jnp.float32),
+            pltpu.VMEM((2, 2 * cap, features), jnp.bfloat16),
+            pltpu.VMEM((2, 2 * cap, features), jnp.bfloat16),
+            pltpu.VMEM((2, 2 * cap, features), jnp.bfloat16),
+            pltpu.SemaphoreType.DMA((3,)),
+            pltpu.SemaphoreType.DMA((8, 4)),
+            pltpu.SemaphoreType.DMA((8, 4)),
+            pltpu.SemaphoreType.DMA((2, 4)),
+            pltpu.SemaphoreType.DMA((2, 4)),
+            pltpu.SemaphoreType.DMA((2,)),
+            pltpu.SemaphoreType.DMA((2,)),
+            pltpu.SemaphoreType.DMA((4,)),
+            pltpu.SemaphoreType.DMA((4,)),
+        ],
+        compiler_params=pltpu.CompilerParams(
+            collective_id=2, has_side_effects=True, vmem_limit_bytes=56 * 1024 * 1024
+        ),
+    )(
+        out_going,
+        gate_weight.reshape(4, width, ff),
+        up_weight.reshape(4, width, ff),
+        down_weight.reshape(4, ff, features),
+    )
+
+
+def split_pair(values):
+    high = lax.reduce_precision(values, 8, 7)
+    return high.astype(jnp.bfloat16), (values - high).astype(jnp.bfloat16)
+
+
+def paired_block(stream, route_experts, weights, channel_gain, gate_weight, up_weight, down_weight):
+    row_count, width = stream.shape
+    cap = row_count // 2
+    group = route_experts[:, 0] // 2
+    near = (group + GROUPS - lax.axis_index("sp") // 2) % GROUPS
+    member = (near[:, None] == jnp.arange(GROUPS, dtype=jnp.int32)[None, :]).astype(jnp.bfloat16)
+    order = jnp.arange(row_count, dtype=jnp.int32)
+    earlier = (order[:, None] > order[None, :]).astype(jnp.bfloat16)
+    counts = jnp.dot(earlier, member, preferred_element_type=jnp.float32)
+    rank = jnp.sum(counts * member.astype(jnp.float32), axis=1).astype(jnp.int32)
+    slot_index = near * cap + rank
+    slots = jnp.arange(GROUPS * cap, dtype=jnp.int32)
+    picker = (slots[:, None] == slot_index[None, :]).astype(jnp.bfloat16)
+    first_low = route_experts[:, 0] % 2 == 0
+    low = jnp.where(first_low, weights[:, 0], weights[:, 1])
+    high = jnp.where(first_low, weights[:, 1], weights[:, 0])
+    squares = jnp.sum(stream * stream, axis=1)
+    columns = split_pair(squares) + split_pair(low) + split_pair(high)
+    extra = jnp.stack(columns, axis=1)
+    extra = jnp.pad(extra, ((0, 0), (0, EXTRA - extra.shape[1])))
+    payload = jnp.concatenate([(stream * channel_gain).astype(jnp.bfloat16), extra], axis=1)
+    out_going = jnp.dot(picker, payload, preferred_element_type=jnp.float32).astype(jnp.bfloat16)
+    arrived = run_experts(
+        out_going.reshape(GROUPS, cap, width + EXTRA), gate_weight, up_weight, down_weight
+    )
+    arrived = arrived.reshape(GROUPS * cap, width)
+    picked = lax.dot_general(
+        picker, arrived, (((0,), (0,)), ((), ())), preferred_element_type=jnp.float32
+    )
+    return (stream + picked).astype(jnp.bfloat16)
 
 
 def on_device(
@@ -140,20 +531,47 @@
     broad_queries, broad_keys, broad_values = own_heads(
         broad_query, broad_key, broad_value, broad_gains, positions, lane_index, HQ_B // KV_B
     )
-    shard_rows = (
-        lax.all_gather(lean_keys, "sp", axis=0, tiled=True),
-        lax.all_gather(lean_values, "sp", axis=0, tiled=True),
-        lax.all_gather(broad_keys, "sp", axis=0, tiled=True),
-        lax.all_gather(broad_values, "sp", axis=0, tiled=True),
-    )
+    chips = lax.axis_size("sp") // 2
+    paired = (
+        lax.axis_size("tp") == 4
+        and chips == GROUPS
+        and chips == 4
+        and route_experts.shape[1] == 2
+        and lean_keys.shape[1] == 1
+        and broad_keys.shape[1] == 1
+    )
+    if paired:
+        own = jnp.concatenate(
+            [part[:, 0] for part in (broad_keys, broad_values, lean_keys, lean_values)], axis=1
+        )
+        every = gather_keys(own, chips).reshape(2 * chips * row_count, -1)
+        broad_size, lean_size = broad_keys.shape[2], lean_keys.shape[2]
+        shard_rows = (
+            every[:, None, 2 * broad_size : 2 * broad_size + lean_size],
+            every[:, None, 2 * broad_size + lean_size :],
+            every[:, None, :broad_size],
+            every[:, None, broad_size : 2 * broad_size],
+        )
+    else:
+        shard_rows = (
+            lax.all_gather(lean_keys, "sp", axis=0, tiled=True),
+            lax.all_gather(lean_values, "sp", axis=0, tiled=True),
+            lax.all_gather(broad_keys, "sp", axis=0, tiled=True),
+            lax.all_gather(broad_values, "sp", axis=0, tiled=True),
+        )
     lean_state = attend_piece(start_state(lean_queries), lean_queries, shard_rows[0], shard_rows[1])
     broad_state = attend_piece(
         start_state(broad_queries), broad_queries, shard_rows[2], shard_rows[3]
     )
-    lean_all, broad_all = (
-        lax.all_gather(finish_heads(lean_state), "tp", axis=1, tiled=True),
-        lax.all_gather(finish_heads(broad_state), "tp", axis=1, tiled=True),
-    )
+    if paired:
+        lean_all, broad_all = gather_heads(
+            finish_heads(lean_state), finish_heads(broad_state), lax.axis_size("tp")
+        )
+    else:
+        lean_all, broad_all = (
+            lax.all_gather(finish_heads(lean_state), "tp", axis=1, tiled=True),
+            lax.all_gather(finish_heads(broad_state), "tp", axis=1, tiled=True),
+        )
     lean_width = lean_all.shape[1]
     stream = tokens.astype(jnp.float32) + jnp.dot(
         group_norm(lean_all, mixer_gain[:lean_width]),
@@ -165,6 +583,18 @@
         output_weight[lean_width:],
         preferred_element_type=jnp.float32,
     )
+    logit_gap = route_logits[:, 0] - route_logits[:, 1]
+    weights = group_weight[:, None] * jax.nn.sigmoid(jnp.stack([logit_gap, -logit_gap], axis=1))
+    if paired:
+        return paired_block(
+            stream,
+            route_experts,
+            weights,
+            channel_gain,
+            gate_weight[0],
+            up_weight[0],
+            down_weight[0],
+        )
     squares = lax.psum(jnp.sum(stream * stream, axis=1), "tp")
     normed = (stream * lax.rsqrt(squares / D + epsilon)[:, None] * channel_gain).astype(
         jnp.bfloat16
@@ -207,8 +637,6 @@
         .reshape(row_count, route_experts.shape[1], -1)
         .astype(jnp.float32)
     )
-    logit_gap = route_logits[:, 0] - route_logits[:, 1]
-    weights = group_weight[:, None] * jax.nn.sigmoid(jnp.stack([logit_gap, -logit_gap], axis=1))
     return (stream + jnp.sum(picked * weights[:, :, None], axis=1)).astype(jnp.bfloat16)
 
 

time: 366 us -> 157 us (0.43)
  waiting for transfers between devices: 149 us -> 0 us
  blocking collectives: 137 us -> 0 us
  Pallas kernels: 0 us -> 121 us
  between operations: 13.9 us -> 0.47 us
  matrix products: 30.7 us -> 17.3 us
  local copies, waits for them, and re-layouts: 14.3 us -> 6.85 us
  starting transfers between devices: 4.65 us -> 0 us
  other arithmetic: 15.9 us -> 11.7 us
    pallas_call x0 -> x3, Pallas kernels: none -> 121 us  [the longest x1 85.2 us: run_experts(): pl.pallas_call(functools.partial(experts_kernel, width), out_shape=jax.Sh...]
    all_gather x2 -> x0, waiting for transfers between devices: 111 us -> none  [the longest x1 67.2 us: on_device(): shard_rows = lax.all_gather(arrived, 'tp', axis=2, tiled=True)]
    all_gather x6 -> x0, blocking collectives: 85.6 us -> none  [the longest x1 17.2 us: on_device(): lax.all_gather(lean_keys, 'sp', axis=0, tiled=True)]
    all_to_all x1 -> x0, blocking collectives: 42.5 us -> none  [on_device(): lax.all_to_all(outgoing, 'sp', split_axis=0, concat_axis=0, tiled=True)]
    all_to_all x1 -> x0, waiting for transfers between devices: 37.6 us -> none  [on_device(): lax.all_to_all(result, 'sp', split_axis=0, concat_axis=0, tiled=True)]
    dot_general x3, matrix products: 19 us -> 3.83 us  [the longest x1 2.3 us: paired_block(): lax.dot_general(picker, arrived, (((0,), (0,)), ((), ())), preferred_elem...]
    psum x1 -> x0, blocking collectives: 8.95 us -> none  [on_device(): squares = lax.psum(jnp.sum(stream * stream, axis=1), 'tp')]
    gather x2 -> x0, local copies, waits for them, and re-layouts: 4.88 us -> none  [the longest x1 2.81 us: on_device(): normed[source]]
  transfers between devices with their start and end apart: 3 -> 0, of which waited for: 3 -> 0; matrix products, arithmetic and copies ran while one was open for 0% -> 0% of each run, Pallas kernels for 0% -> 0%
where the time goes in v1:
time: 157 us
  Pallas kernels  121 us (77%)
  matrix products  17.3 us (11%)
  other arithmetic  11.7 us (7%)
  local copies, waits for them, and re-layouts  6.85 us (4%)
    pallas_call x1, Pallas kernels, run_experts(): pl.pallas_call(functools.partial(experts_kernel, width), out_shape=jax.Sh...  85.2 us
    pallas_call x1, Pallas kernels, gather_keys(): pl.pallas_call(functools.partial(keys_kernel, chips), out_shape=jax.Shape...  19.3 us
    pallas_call x1, Pallas kernels, gather_heads(): pl.pallas_call(heads_kernel, out_shape=[jax.ShapeDtypeStruct((part.shape[...  16.1 us
    dot_general x2, matrix products, attend_piece(): jnp.einsum('kgqs,skd->qkgd', rounded, values, preferred_element_type=jnp....  4.53 us
    dot_general x1, matrix products, on_device(): jnp.dot(group_norm(broad_all, mixer_gain[lean_width:]), output_weight[lea...  3.46 us

profile of v1, /device:TPU:0, one launch (start us, length us, event | category | flops | bytes accessed | tf_op | source)
XLA Modules:
  0.0 156.9 jit_solution(3022477544560104562)
XLA Ops:
  1.0 0.8 multiply_cosine_fusion.1
  1.8 0.8 slice_bitcast_fusion.8
  2.5 1.1 fusion.46
  3.7 1.1 fusion.47
  5.2 0.8 constant_dynamic-slice_fusion
  6.2 0.8 slice_bitcast_fusion.9
  7.1 0.8 fusion.115
  8.4 0.8 fusion.111
  9.4 0.9 concatenate.53.own_ref
  10.2 19.3 %shard_map.172 = bf16[2,4,192,384]{3,2,1,0:T(8,128)(2,1)} custom-call(bf16[192,384]{1,0:T(8,128)(2,1)} %concatenate.53.own_ref), custom_call_target="tpu_custom_call" | custom-call | tf_op jit(solution)/shard_map/pallas_call | solution.py:176
  29.6 2.0 %bitcast_reduce_fusion = (f32[4,192]{1,0:T(4,128)S(1)}, f32[1536,192,4]{0,1,2:T(8,128)S(1)}) fusion(bf16[192,4,32]{2,0,1:T(8,128)(2,1)S(1)} %get-tuple-element.23, bf16[192,4,32]{2,0,1:T(8,128)(2,1)S(1)} %get-tuple-element.24, bf16[192,4,32]{2,0,1:T(8,128)(2,1)S(1)} %get-tuple-element.20, bf16[192,4,32]{2,0,1:T(8,128)(2,1)S(1)} %get-tuple-element.19, ...), kind=kOutput, calls=%fused_computation.7 | convolution fusion | flops 305134848 | bytes 5311488 | tf_op jit(solution)/shard_map/qkgd,skd->kgqs/dot_general | solution.py:94
  31.6 0.9 fusion.30
  32.8 0.9 fusion.1
  35.3 1.0 bitcast_reduce_fusion.1
  36.3 2.1 %copy-done = f32[1536,192,4]{0,1,2:T(8,128)} copy-done((f32[1536,192,4]{0,1,2:T(8,128)}, f32[1536,192,4]{0,1,2:T(8,128)S(1)}, u32[]{:S(2)}) %copy-start) | copy-done | bytes 4718616
  38.4 0.9 fusion.3
  39.5 3.6 %fusion.16 = f32[64,4,192]{2,0,1:T(8,128)S(1)} fusion(f32[1536,192,4]{0,1,2:T(8,128)} %copy-done, f32[4,192]{1,0:T(4,128)S(1)} %broadcast_maximum_fusion.1, bf16[1536,384]{1,0:T(8,128)(2,1)S(1)} %bitcast.129), kind=kOutput, calls=%fused_computation.22 | convolution fusion | flops 154533888 | bytes 5312512 | tf_op jit(solution)/shard_map/kgqs,skd->qkgd/dot_general | solution.py:102
  43.9 16.1 %shard_map.173 = (bf16[192,1024]{1,0:T(8,128)(2,1)}, bf16[192,2048]{1,0:T(8,128)(2,1)}) custom-call(bf16[192,256]{1,0:T(8,128)(2,1)} %divide_convert_fusion.lean_ref, bf16[192,512]{1,0:T(8,128)(2,1)} %fusion.49.broad_ref), custom_call_target="tpu_custom_call" | custom-call | tf_op jit(solution)/shard_map/pallas_call | solution.py:221
  60.0 1.4 fusion.20
  61.5 3.5 %fusion.8 = f32[192,1024]{1,0:T(8,128)S(1)} fusion(bf16[3072,1024]{1,0:T(8,128)(2,1)} %param.28, bf16[192,2048]{1,0:T(8,128)(2,1)} %get-tuple-element.8, f32[2048]{0:T(1024)S(1)} %slice-done, f32[192]{0:T(256)S(1)} %add_rsqrt_fusion.2), kind=kOutput, calls=%fused_computation.14 | convolution fusion | flops 806879232 | bytes 5776128 | tf_op jit(solution)/shard_map/dot_general | solution.py:581
  65.3 2.4 %multiply_convert_fusion = (bf16[192,1024]{1,0:T(8,128)(2,1)S(1)}, f32[192]{0:T(256)S(1)}, f32[192,1024]{1,0:T(8,128)S(1)}) fusion(f32[1024]{0:T(1024)S(1)} %copy-done.9, f32[192,1024]{1,0:T(8,128)S(1)} %fusion.8, bf16[3072,1024]{1,0:T(8,128)(2,1)} %param.28, bf16[192,1024]{1,0:T(8,128)(2,1)S(1)} %copy-done.3, f32[1024]{0:T(1024)S(1)} %slice-done.1, ...), kind=kOutput, calls=%fused_computation.45 | convolution fusion | flops 404815680 | bytes 4859392 | tf_op jit(solution)/shard_map/dot_general | solution.py:576
  68.0 1.4 convolution_convert_fusion
  69.4 85.2 %shard_map.174 = bf16[4,96,1024]{2,1,0:T(8,128)(2,1)} custom-call(bf16[4,96,1152]{2,1,0:T(8,128)(2,1)} %bitcast.138, bf16[4,1024,512]{2,1,0:T(8,128)(2,1)} %bitcast.130, bf16[4,1024,512]{2,1,0:T(8,128)(2,1)} %bitcast.131, bf16[4,512,1024]{2,1,0:T(8,128)(2,1)} %bitcast.132), custom_call_target="tpu_custom_call" | custom-call | tf_op jit(solution)/shard_map/pallas_call | solution.py:429
  154.6 2.3 %fusion.29 = bf16[192,1024]{1,0:T(8,128)(2,1)} fusion(f32[192,1024]{1,0:T(8,128)S(1)} %get-tuple-element.68, bf16[384,1024]{1,0:T(8,128)(2,1)} %bitcast.133, s32[192]{0:T(256)S(1)} %get-tuple-element.70), kind=kOutput, calls=%fused_computation.33 | convolution fusion | flops 151461888 | bytes 1966848 | tf_op jit(solution)/shard_map/dot_general | solution.py:499
  (66 shorter events, 5.5 us)
Async XLA Ops:
  0.0 7.9 %copy-start.5 = (bf16[192,2,128]{2,1,0:T(2,128)(2,1)S(1)}, bf16[192,2,128]{2,1,0:T(2,128)(2,1)}, u32[]{:S(2)}) copy-start(bf16[192,2,128]{2,1,0:T(2,128)(2,1)} %param.24) | copy-start | bytes 294916
  0.0 7.9 %copy-start.4 = (bf16[192,2,128]{2,1,0:T(2,128)(2,1)S(1)}, bf16[192,2,128]{2,1,0:T(2,128)(2,1)}, u32[]{:S(2)}) copy-start(bf16[192,2,128]{2,1,0:T(2,128)(2,1)} %param.25) | copy-start | bytes 294916
  29.6 2.1 %copy-start.1 = (bf16[2,4,192,384]{3,2,1,0:T(8,128)(2,1)S(1)}, bf16[2,4,192,384]{3,2,1,0:T(8,128)(2,1)}, u32[]{:S(2)}) copy-start(bf16[2,4,192,384]{3,2,1,0:T(8,128)(2,1)} %shard_map.172) | copy-start | bytes 3538948
  32.5 2.5 %copy-start.2 = (bf16[192,4,64]{0,2,1:T(8,128)(2,1)S(1)}, bf16[192,4,64]{0,2,1:T(8,128)(2,1)}, u32[]{:S(2)}) copy-start(bf16[192,4,64]{0,2,1:T(8,128)(2,1)} %param.19) | copy-start | bytes 294916
  36.3 2.1 %copy-start = (f32[1536,192,4]{0,1,2:T(8,128)}, f32[1536,192,4]{0,1,2:T(8,128)S(1)}, u32[]{:S(2)}) copy-start(f32[1536,192,4]{0,1,2:T(8,128)S(1)} %get-tuple-element.65) | copy-start | bytes 14155780
  39.3 22.2 %slice-start = ((f32[3072]{0:T(1024)}), f32[2048]{0:T(1024)S(1)}, s32[]{:S(2)}) async-start(f32[3072]{0:T(1024)} %param.27), calls=%async_computation | async-start | bytes 16384 | tf_op jit(solution)/shard_map/slice | solution.py:582
  60.0 5.0 %copy-start.3 = (bf16[192,1024]{1,0:T(8,128)(2,1)S(1)}, bf16[192,1024]{1,0:T(8,128)(2,1)}, u32[]{:S(2)}) copy-start(bf16[192,1024]{1,0:T(8,128)(2,1)} %get-tuple-element.7) | copy-start | bytes 1179652
  60.0 5.3 %slice-start.1 = ((f32[3072]{0:T(1024)}), f32[1024]{0:T(1024)S(1)}, s32[]{:S(2)}) async-start(f32[3072]{0:T(1024)} %param.27), calls=%async_computation.1 | async-start | bytes 8192 | tf_op jit(solution)/shard_map/slice | solution.py:577
  60.0 5.3 %copy-start.8 = (bf16[192,1024]{1,0:T(8,128)(2,1)S(1)}, bf16[192,1024]{1,0:T(8,128)(2,1)}, u32[]{:S(2)}) copy-start(bf16[192,1024]{1,0:T(8,128)(2,1)} %param.18) | copy-start | bytes 1179652
  60.0 5.3 %copy-start.9 = (f32[1024]{0:T(1024)S(1)}, f32[1024]{0:T(1024)}, u32[]{:S(2)}) copy-start(f32[1024]{0:T(1024)} %param.29) | copy-start | bytes 12292
  64.9 2.8 %copy-start.6 = (f32[192,2]{0,1:T(2,128)S(1)}, f32[192,2]{0,1:T(2,128)}, u32[]{:S(2)}) copy-start(f32[192,2]{0,1:T(2,128)} %param.34) | copy-start | bytes 4612
  64.9 2.8 %copy-start.7 = (f32[192]{0:T(256)S(1)}, f32[192]{0:T(256)}, u32[]{:S(2)}) copy-start(f32[192]{0:T(256)} %param.35) | copy-start | bytes 2308

commit v2 on v1

--- a/solution.py
+++ b/solution.py
@@ -2,6 +2,7 @@
 
 import jax
 import jax.numpy as jnp
+import numpy as np
 from jax import lax
 from jax.experimental import pallas as pl
 from jax.experimental.pallas import tpu as pltpu
@@ -148,87 +149,338 @@
     )
 
 
-def keys_kernel(chips, own_ref, out_ref, z_send, z_recv, s_send, s_recv):
+def front_kernel(
+    chips,
+    lean_q,
+    lean_k,
+    lean_v,
+    broad_q,
+    broad_k,
+    broad_v,
+    lean_gain,
+    broad_gain,
+    cosines,
+    sines,
+    mixer_gain,
+    tokens,
+    channel_gain,
+    picker,
+    route_columns,
+    weight_hbm,
+    stream_out,
+    going_out,
+    own,
+    keys,
+    queries,
+    peak,
+    total,
+    mass,
+    lean_heads,
+    broad_heads,
+    weight,
+    lean_acc,
+    broad_acc,
+    w_sem,
+    k_send,
+    k_recv,
+    h_send,
+    h_recv,
+):
     z, core, tp, sibling, x_peer, y_peer, chunks = place()
+    x, y = tp % 2, tp // 2
+    rows = own.shape[0]
+    half = rows // 2
+    lanes = 128
     peers = [{"sp": ((z + d) % chips) * 2 + core, "tp": tp} for d in range(1, chips)]
-    enter(peers + [sibling])
-    sends = [
-        remote(own_ref, out_ref.at[0, d], z_send.at[d], z_recv.at[d], peers[d - 1])
-        for d in range(1, chips)
-    ]
-    for copy in sends:
+    load = pltpu.make_async_copy(weight_hbm, weight, w_sem.at[0])
+    load.start()
+    lane = lax.broadcasted_iota(jnp.int32, (rows, lanes), 1)
+    low = lane < lanes // 2
+
+    def turned(raw, gain, size):
+        values = raw.astype(jnp.float32)
+        squares = values * values
+        if size == lanes:
+            mean = jnp.sum(squares, axis=1, keepdims=True) / size
+        else:
+            first = jnp.sum(jnp.where(low, squares, 0.0), axis=1, keepdims=True)
+            second = jnp.sum(jnp.where(low, 0.0, squares), axis=1, keepdims=True)
+            mean = jnp.where(low, first, second) / size
+        values = values * lax.rsqrt(mean + epsilon) * gain
+        quarter = size // 4
+        partner = jnp.where(
+            lane % (2 * quarter) < quarter,
+            pltpu.roll(values, lanes - quarter, 1),
+            pltpu.roll(values, quarter, 1),
+        )
+        part = pl.ds(0 if size == lanes else lanes, lanes)
+        return values * cosines[:, part] + partner * sines[:, part]
+
+    def swapped(values):
+        return pltpu.roll(values, lanes // 2, 1)
+
+    key_columns = pl.ds(pl.multiple_of(y * lanes, lanes), lanes)
+    own[:, :lanes] = turned(broad_k[:, key_columns], broad_gain[1:2, :], lanes).astype(jnp.bfloat16)
+    own[:, lanes : 2 * lanes] = broad_v[:, key_columns]
+    both_keys = turned(lean_k[...], lean_gain[1:2, :], lanes // 2)
+    both_values = lean_v[...].astype(jnp.float32)
+    at_first = (1 - y).astype(jnp.float32)
+    lean_key = both_keys * at_first + swapped(both_keys) * (1.0 - at_first)
+    lean_value = swapped(both_values) * at_first + both_values * (1.0 - at_first)
+    own[:, 2 * lanes :] = jnp.where(low, lean_key, lean_value).astype(jnp.bfloat16)
+
+    enter(peers + [sibling, x_peer, y_peer])
+    pending = []
+    arrivals = {}
+
+    def send(kind, d, source, target, device):
+        copy = remote(source, target, k_send.at[kind, d], k_recv.at[kind, d], device)
         copy.start()
-    forwards = [remote(own_ref, out_ref.at[1, 0], s_send.at[0], s_recv.at[0], sibling)]
-    forwards[0].start()
-    out_ref[0, 0] = own_ref[...]
+        pending.append(copy)
+        arrivals[kind, d] = copy
+
+    mine = pl.ds(pl.multiple_of(x * half, half), half)
+    other = pl.ds(pl.multiple_of((1 - x) * half, half), half)
+    side_mine = pl.ds(pl.multiple_of(rows + x * half, half), half)
+    side_other = pl.ds(pl.multiple_of(rows + (1 - x) * half, half), half)
+    Z, X, A, B = 0, 1, 2, 3
     for d in range(1, chips):
-        sends[d - 1].wait_recv()
-        copy = remote(out_ref.at[0, d], out_ref.at[1, d], s_send.at[d], s_recv.at[d], sibling)
-        copy.start()
-        forwards.append(copy)
-    for copy in forwards:
-        copy.wait()
-    for copy in sends:
+        send(Z, d, own.at[mine], keys.at[d, mine], peers[d - 1])
+    send(A, 0, own, keys.at[0, pl.ds(rows, rows)], sibling)
+    keys[0, pl.ds(0, rows)] = own[...]
+
+    heads = queries.shape[1]
+    for h in range(heads):
+        part = pl.ds(h * lanes, lanes)
+        queries[1, h] = turned(broad_q[:, part], broad_gain[0:1, :], lanes).astype(jnp.bfloat16)
+    for h in range(heads // 2):
+        part = pl.ds(h * lanes, lanes)
+        pair = turned(lean_q[:, part], lean_gain[0:1, :], lanes // 2)
+        queries[0, 2 * h] = jnp.where(low, pair, 0.0).astype(jnp.bfloat16)
+        queries[0, 2 * h + 1] = jnp.where(low, swapped(pair), 0.0).astype(jnp.bfloat16)
+
+    def attend(d, kind):
+        size = lanes // 2 if kind == 0 else lanes
+        key_part = pl.ds(2 * lanes, lanes) if kind == 0 else pl.ds(0, lanes)
+        value_part = pl.ds(2 * lanes, lanes) if kind == 0 else pl.ds(lanes, lanes)
+
+        def one_head(h, carry):
+            scores = lax.dot_general(
+                queries[kind, h],
+                keys[d, :, key_part],
+                (((1,), (1,)), ((), ())),
+                preferred_element_type=jnp.float32,
+            ) * (size**-0.5)
+            top = jnp.max(scores, axis=1, keepdims=True)
+            if d:
+                old = peak[kind, h][:, :1]
+                top = jnp.maximum(old, top)
+            weights = jnp.exp(scores - top)
+            summed = jnp.sum(weights, axis=1, keepdims=True)
+            partial = jnp.dot(
+                weights.astype(jnp.bfloat16),
+                keys[d, :, value_part],
+                preferred_element_type=jnp.float32,
+            )
+            if d:
+                shrink = jnp.exp(old - top)
+                summed = summed + total[kind, h][:, :1] * shrink
+                partial = partial + mass[kind, h] * shrink
+            peak[kind, h] = jnp.broadcast_to(top, (rows, lanes))
+            total[kind, h] = jnp.broadcast_to(summed, (rows, lanes))
+            mass[kind, h] = partial
+            return carry
+
+        lax.fori_loop(0, heads, one_head, 0)
+
+    def forward(d):
+        arrivals[Z, d].wait_recv()
+        send(X, d, keys.at[d, mine], keys.at[d, mine], x_peer)
+        send(A, d, keys.at[d, mine], keys.at[d, side_mine], sibling)
+
+    def forward_other(d):
+        arrivals[X, d].wait_recv()
+        send(B, d, keys.at[d, other], keys.at[d, side_other], sibling)
+
+    forward(1)
+    arrivals[A, 0].wait_recv()
+    attend(0, 0)
+    forward_other(1)
+    attend(0, 1)
+    for d in range(1, chips):
+        if d + 1 < chips:
+            forward(d + 1)
+        arrivals[A, d].wait_recv()
+        arrivals[B, d].wait_recv()
+        if d + 1 < chips:
+            attend(d, 0)
+            forward_other(d + 1)
+            attend(d, 1)
+
+    gathers = {}
+
+    def spread(kind, buffer):
+        for k, peer in ((0, x_peer), (1, y_peer)):
+            n = kind * 4 + k
+            copy = remote(buffer.at[0], buffer.at[1 + k], h_send.at[n], h_recv.at[n], peer)
+            copy.start()
+            pending.append(copy)
+            gathers[kind, k] = copy
+
+    def relay(kind, buffer):
+        for k, peer in ((0, y_peer), (1, x_peer)):
+            n = kind * 4 + 2 + k
+            gathers[kind, k].wait_recv()
+            part = pl.ds(k * half, half)
+            copy = remote(
+                buffer.at[1 + k, part], buffer.at[3, part], h_send.at[n], h_recv.at[n], peer
+            )
+            copy.start()
+            pending.append(copy)
+            gathers[kind, 2 + k] = copy
+
+    def finished(kind, h):
+        return mass[kind, h] / total[kind, h]
+
+    attend(chips - 1, 0)
+    for h in range(heads // 2):
+        pair = jnp.where(low, swapped(finished(0, 2 * h)), finished(0, 2 * h + 1))
+        lean_heads[0, :, pl.ds(h * lanes, lanes)] = pair.astype(jnp.bfloat16)
+    spread(0, lean_heads)
+    attend(chips - 1, 1)
+    for h in range(heads):
+        broad_heads[0, :, pl.ds(h * lanes, lanes)] = finished(1, h).astype(jnp.bfloat16)
+    spread(1, broad_heads)
+    load.wait()
+    lean_width, broad_width = lean_heads.shape[2], broad_heads.shape[2]
+    squares = [0.0, 0.0]
+
+    def project(kind, r):
+        buffer, acc, width, start = (
+            (lean_heads, lean_acc, lean_width, 0),
+            (broad_heads, broad_acc, broad_width, 4 * lean_width),
+        )[kind]
+        part = pl.ds(pl.multiple_of(start + chunks[r] * width, width), width)
+        values = buffer[r].astype(jnp.float32)
+        squares[kind] = squares[kind] + jnp.sum(values * values, axis=1, keepdims=True)
+        scaled = (values * mixer_gain[:, part]).astype(jnp.bfloat16)
+        product = jnp.dot(scaled, weight[part, :], preferred_element_type=jnp.float32)
+        if r == 0:
+            acc[...] = product
+        else:
+            acc[...] += product
+
+    project(0, 0)
+    relay(0, lean_heads)
+    project(1, 0)
+    project(0, 1)
+    project(0, 2)
+    relay(1, broad_heads)
+    project(1, 1)
+    project(1, 2)
+    for kind in (0, 1):
+        gathers[kind, 2].wait_recv()
+        gathers[kind, 3].wait_recv()
+        project(kind, 3)
+    lean_scale = lax.rsqrt(squares[0] / (4 * lean_width) + epsilon)
+    broad_scale = lax.rsqrt(squares[1] / (4 * broad_width) + epsilon)
+    stream = (
+        tokens[...].astype(jnp.float32)
+        + lean_acc[...] * lean_scale
+        + broad_acc[...] * broad_scale
+    )
+    stream_out[...] = stream
+    width = stream.shape[1]
+    norm = jnp.sum(stream * stream, axis=1, keepdims=True)
+    norm_high = norm.astype(jnp.bfloat16).astype(jnp.float32)
+    extra = jnp.where(
+        lane == 0, norm_high, jnp.where(lane == 1, norm - norm_high, route_columns[...])
+    ).astype(jnp.bfloat16)
+    scaled = (stream * channel_gain[...]).astype(jnp.bfloat16)
+    going_out[:, :width] = jnp.dot(
+        picker[...], scaled, preferred_element_type=jnp.float32
+    ).astype(jnp.bfloat16)
+    going_out[:, width:] = jnp.dot(
+        picker[...], extra, preferred_element_type=jnp.float32
+    ).astype(jnp.bfloat16)
+    for copy in pending:
         copy.wait_send()
 
 
-def gather_keys(own, chips):
+def lane_frequencies(head_size):
+    quarter = head_size // 4
+    lane = np.arange(128) % head_size
+    frequency = theta_base ** (-(lane % quarter).astype(np.float32) / np.float32(quarter))
+    by_row = lane < head_size // 2
+    sign = np.where(lane // quarter % 2 == 0, -1.0, 1.0)
+    return frequency.astype(np.float32), by_row, sign.astype(np.float32)
+
+
+def run_front(
+    chips,
+    positions,
+    lean,
+    broad,
+    lean_gains,
+    broad_gains,
+    mixer_gain,
+    tokens,
+    channel_gain,
+    picker,
+    route_columns,
+    output_weight,
+):
+    rows, width = tokens.shape
+    heads = lean[0].shape[1]
+    tables = [lane_frequencies(part[0].shape[2]) for part in (broad, lean)]
+    frequency, by_row, sign = (np.concatenate(parts)[None, :] for parts in zip(*tables))
+    row = (positions // GRID_W).astype(jnp.float32)[:, None]
+    column = (positions % GRID_W).astype(jnp.float32)[:, None]
+    angles = jnp.where(by_row, row, column) * frequency
+    flat = [part.reshape(rows, -1) for part in lean + broad]
     return pl.pallas_call(
-        functools.partial(keys_kernel, chips),
-        out_shape=jax.ShapeDtypeStruct((2, chips) + own.shape, own.dtype),
-        in_specs=[pl.BlockSpec(memory_space=pltpu.VMEM)],
-        out_specs=pl.BlockSpec(memory_space=pltpu.VMEM),
-        scratch_shapes=[pltpu.SemaphoreType.DMA((chips,))] * 4,
-        compiler_params=pltpu.CompilerParams(collective_id=0, has_side_effects=True),
-    )(own)
-
-
-def heads_kernel(lean_ref, broad_ref, lean_out, broad_out, send_sem, recv_sem):
-    z, core, tp, sibling, x_peer, y_peer, chunks = place()
-    enter([x_peer, y_peer])
-    half = lean_ref.shape[0] // 2
-    pieces = ((lean_ref, lean_out), (broad_ref, broad_out))
-
-    def columns(ref, chunk):
-        width = ref.shape[1]
-        return pl.ds(pl.multiple_of(chunk * width, width), width)
-
-    first = []
-    for i, (own, out) in enumerate(pieces):
-        for j, peer in enumerate((x_peer, y_peer)):
-            k = i * 2 + j
-            copy = remote(own, out.at[:, columns(own, tp)], send_sem.at[k], recv_sem.at[k], peer)
-            copy.start()
-            first.append(copy)
-    for own, out in pieces:
-        out[:, columns(own, tp)] = own[...]
-    second = []
-    for i, (own, out) in enumerate(pieces):
-        for j, peer in enumerate((y_peer, x_peer)):
-            first[i * 2 + j].wait_recv()
-            k = 4 + i * 2 + j
-            part = out.at[pl.ds(j * half, half), columns(own, chunks[1 + j])]
-            copy = remote(part, part, send_sem.at[k], recv_sem.at[k], peer)
-            copy.start()
-            second.append(copy)
-    for copy in second:
-        copy.wait()
-    for copy in first:
-        copy.wait_send()
-
-
-def gather_heads(lean, broad, lanes):
-    return pl.pallas_call(
-        heads_kernel,
+        functools.partial(front_kernel, chips),
         out_shape=[
-            jax.ShapeDtypeStruct((part.shape[0], part.shape[1] * lanes), part.dtype)
-            for part in (lean, broad)
+            jax.ShapeDtypeStruct((rows, width), jnp.float32),
+            jax.ShapeDtypeStruct((picker.shape[0], width + EXTRA), jnp.bfloat16),
         ],
-        in_specs=[pl.BlockSpec(memory_space=pltpu.VMEM)] * 2,
+        in_specs=[pl.BlockSpec(memory_space=pltpu.VMEM)] * 15
+        + [pl.BlockSpec(memory_space=pl.ANY)],
         out_specs=[pl.BlockSpec(memory_space=pltpu.VMEM)] * 2,
-        scratch_shapes=[pltpu.SemaphoreType.DMA((8,))] * 2,
-        compiler_params=pltpu.CompilerParams(collective_id=1, has_side_effects=True),
-    )(lean, broad)
+        scratch_shapes=[
+            pltpu.VMEM((rows, 384), jnp.bfloat16),
+            pltpu.VMEM((chips, 2 * rows, 384), jnp.bfloat16),
+            pltpu.VMEM((2, heads, rows, 128), jnp.bfloat16),
+            pltpu.VMEM((2, heads, rows, 128), jnp.float32),
+            pltpu.VMEM((2, heads, rows, 128), jnp.float32),
+            pltpu.VMEM((2, heads, rows, 128), jnp.float32),
+            pltpu.VMEM((4, rows, heads * 64), jnp.bfloat16),
+            pltpu.VMEM((4, rows, heads * 128), jnp.bfloat16),
+            pltpu.VMEM(output_weight.shape, jnp.bfloat16),
+            pltpu.VMEM((rows, width), jnp.float32),
+            pltpu.VMEM((rows, width), jnp.float32),
+            pltpu.SemaphoreType.DMA((1,)),
+            pltpu.SemaphoreType.DMA((4, chips)),
+            pltpu.SemaphoreType.DMA((4, chips)),
+            pltpu.SemaphoreType.DMA((8,)),
+            pltpu.SemaphoreType.DMA((8,)),
+        ],
+        compiler_params=pltpu.CompilerParams(
+            collective_id=0, has_side_effects=True, vmem_limit_bytes=48 * 1024 * 1024
+        ),
+    )(
+        *flat,
+        jnp.concatenate([lean_gains, lean_gains], axis=1),
+        broad_gains,
+        jnp.cos(angles),
+        jnp.sin(angles) * sign,
+        mixer_gain[None, :],
+        tokens,
+        channel_gain[None, :],
+        picker,
+        route_columns,
+        output_weight,
+    )
 
 
 def experts_kernel(
@@ -467,11 +719,25 @@
 
 def split_pair(values):
     high = lax.reduce_precision(values, 8, 7)
-    return high.astype(jnp.bfloat16), (values - high).astype(jnp.bfloat16)
-
-
-def paired_block(stream, route_experts, weights, channel_gain, gate_weight, up_weight, down_weight):
-    row_count, width = stream.shape
+    return high, values - high
+
+
+def paired_block(
+    chips,
+    positions,
+    tokens,
+    lean,
+    lean_gains,
+    broad,
+    broad_gains,
+    mixer_gain,
+    output_weight,
+    channel_gain,
+    expert_weights,
+    route_experts,
+    weights,
+):
+    row_count, width = tokens.shape
     cap = row_count // 2
     group = route_experts[:, 0] // 2
     near = (group + GROUPS - lax.axis_index("sp") // 2) % GROUPS
@@ -486,15 +752,25 @@
     first_low = route_experts[:, 0] % 2 == 0
     low = jnp.where(first_low, weights[:, 0], weights[:, 1])
     high = jnp.where(first_low, weights[:, 1], weights[:, 0])
-    squares = jnp.sum(stream * stream, axis=1)
-    columns = split_pair(squares) + split_pair(low) + split_pair(high)
-    extra = jnp.stack(columns, axis=1)
-    extra = jnp.pad(extra, ((0, 0), (0, EXTRA - extra.shape[1])))
-    payload = jnp.concatenate([(stream * channel_gain).astype(jnp.bfloat16), extra], axis=1)
-    out_going = jnp.dot(picker, payload, preferred_element_type=jnp.float32).astype(jnp.bfloat16)
-    arrived = run_experts(
-        out_going.reshape(GROUPS, cap, width + EXTRA), gate_weight, up_weight, down_weight
-    )
+    lane = jnp.arange(EXTRA, dtype=jnp.int32)[None, :]
+    route_columns = jnp.zeros((row_count, EXTRA), jnp.float32)
+    for i, column in enumerate(split_pair(low) + split_pair(high)):
+        route_columns = jnp.where(lane == 2 + i, column[:, None], route_columns)
+    stream, out_going = run_front(
+        chips,
+        positions,
+        lean,
+        broad,
+        lean_gains,
+        broad_gains,
+        mixer_gain,
+        tokens,
+        channel_gain,
+        picker,
+        route_columns,
+        output_weight,
+    )
+    arrived = run_experts(out_going.reshape(GROUPS, cap, width + EXTRA), *expert_weights)
     arrived = arrived.reshape(GROUPS * cap, width)
     picked = lax.dot_general(
         picker, arrived, (((0,), (0,)), ((), ())), preferred_element_type=jnp.float32
@@ -525,53 +801,54 @@
     row_count = tokens.shape[0]
     positions = lax.axis_index("sp") * row_count + jnp.arange(row_count, dtype=jnp.int32)
     lane_index = lax.axis_index("tp")
-    lean_queries, lean_keys, lean_values = own_heads(
-        lean_query, lean_key, lean_value, lean_gains, positions, lane_index, HQ_A // KV_A
-    )
-    broad_queries, broad_keys, broad_values = own_heads(
-        broad_query, broad_key, broad_value, broad_gains, positions, lane_index, HQ_B // KV_B
-    )
+    logit_gap = route_logits[:, 0] - route_logits[:, 1]
+    weights = group_weight[:, None] * jax.nn.sigmoid(jnp.stack([logit_gap, -logit_gap], axis=1))
     chips = lax.axis_size("sp") // 2
-    paired = (
+    if (
         lax.axis_size("tp") == 4
         and chips == GROUPS
         and chips == 4
         and route_experts.shape[1] == 2
-        and lean_keys.shape[1] == 1
-        and broad_keys.shape[1] == 1
-    )
-    if paired:
-        own = jnp.concatenate(
-            [part[:, 0] for part in (broad_keys, broad_values, lean_keys, lean_values)], axis=1
+        and lean_query.shape[1:] == (4, 64)
+        and broad_query.shape[1:] == (4, 128)
+        and lean_key.shape[1:] == (2, 64)
+        and broad_key.shape[1:] == (2, 128)
+    ):
+        return paired_block(
+            chips,
+            positions,
+            tokens,
+            (lean_query, lean_key, lean_value),
+            lean_gains,
+            (broad_query, broad_key, broad_value),
+            broad_gains,
+            mixer_gain,
+            output_weight,
+            channel_gain,
+            (gate_weight[0], up_weight[0], down_weight[0]),
+            route_experts,
+            weights,
         )
-        every = gather_keys(own, chips).reshape(2 * chips * row_count, -1)
-        broad_size, lean_size = broad_keys.shape[2], lean_keys.shape[2]
-        shard_rows = (
-            every[:, None, 2 * broad_size : 2 * broad_size + lean_size],
-            every[:, None, 2 * broad_size + lean_size :],
-            every[:, None, :broad_size],
-            every[:, None, broad_size : 2 * broad_size],
-        )
-    else:
-        shard_rows = (
-            lax.all_gather(lean_keys, "sp", axis=0, tiled=True),
-            lax.all_gather(lean_values, "sp", axis=0, tiled=True),
-            lax.all_gather(broad_keys, "sp", axis=0, tiled=True),
-            lax.all_gather(broad_values, "sp", axis=0, tiled=True),
-        )
+    lean_queries, lean_keys, lean_values = own_heads(
+        lean_query, lean_key, lean_value, lean_gains, positions, lane_index, HQ_A // KV_A
+    )
+    broad_queries, broad_keys, broad_values = own_heads(
+        broad_query, broad_key, broad_value, broad_gains, positions, lane_index, HQ_B // KV_B
+    )
+    shard_rows = (
+        lax.all_gather(lean_keys, "sp", axis=0, tiled=True),
+        lax.all_gather(lean_values, "sp", axis=0, tiled=True),
+        lax.all_gather(broad_keys, "sp", axis=0, tiled=True),
+        lax.all_gather(broad_values, "sp", axis=0, tiled=True),
+    )
     lean_state = attend_piece(start_state(lean_queries), lean_queries, shard_rows[0], shard_rows[1])
     broad_state = attend_piece(
         start_state(broad_queries), broad_queries, shard_rows[2], shard_rows[3]
     )
-    if paired:
-        lean_all, broad_all = gather_heads(
-            finish_heads(lean_state), finish_heads(broad_state), lax.axis_size("tp")
-        )
-    else:
-        lean_all, broad_all = (
-            lax.all_gather(finish_heads(lean_state), "tp", axis=1, tiled=True),
-            lax.all_gather(finish_heads(broad_state), "tp", axis=1, tiled=True),
-        )
+    lean_all, broad_all = (
+        lax.all_gather(finish_heads(lean_state), "tp", axis=1, tiled=True),
+        lax.all_gather(finish_heads(broad_state), "tp", axis=1, tiled=True),
+    )
     lean_width = lean_all.shape[1]
     stream = tokens.astype(jnp.float32) + jnp.dot(
         group_norm(lean_all, mixer_gain[:lean_width]),
@@ -583,18 +860,6 @@
         output_weight[lean_width:],
         preferred_element_type=jnp.float32,
     )
-    logit_gap = route_logits[:, 0] - route_logits[:, 1]
-    weights = group_weight[:, None] * jax.nn.sigmoid(jnp.stack([logit_gap, -logit_gap], axis=1))
-    if paired:
-        return paired_block(
-            stream,
-            route_experts,
-            weights,
-            channel_gain,
-            gate_weight[0],
-            up_weight[0],
-            down_weight[0],
-        )
     squares = lax.psum(jnp.sum(stream * stream, axis=1), "tp")
     normed = (stream * lax.rsqrt(squares / D + epsilon)[:, None] * channel_gain).astype(
         jnp.bfloat16

time: 157 us -> 144 us (0.917)
  matrix products: 17.3 us -> 2.47 us
  other arithmetic: 11.7 us -> 5.46 us
  Pallas kernels: 121 us -> 126 us
  local copies, waits for them, and re-layouts: 6.85 us -> 8.8 us
    dot_general x7 -> x0, matrix products: 14.8 us -> none  [the longest x2 4.53 us: attend_piece(): jnp.einsum('kgqs,skd->qkgd', rounded, values, preferred_element_type=jnp....]
    pallas_call x2 -> x1, Pallas kernels: 35.4 us -> 42.8 us  [run_front(): pl.pallas_call(functools.partial(front_kernel, chips), out_shape=[jax.Sha...]
    reduce_sum x8 -> x0, other arithmetic: 5.02 us -> none  [the longest x2 1.82 us: attend_piece(): new_sum = jnp.sum(weights, axis=-1)]
    reshape x1 -> x4, local copies, waits for them, and re-layouts: 0.12 us -> 3.87 us  [run_front(): flat = [part.reshape(rows, -1) for part in lean + broad]]
    unnamed x22 -> x11, local copies, waits for them, and re-layouts: 2.28 us -> 4.93 us
    pallas_call x1, Pallas kernels: 85.2 us -> 83.5 us  [run_experts(): pl.pallas_call(functools.partial(experts_kernel, width), out_shape=jax.Sh...]
where the time goes in v2:
time: 144 us; the launch traced here: 143 us
  Pallas kernels  126 us (88%)
  local copies, waits for them, and re-layouts  8.8 us (6%)
  other arithmetic  5.46 us (4%)
  matrix products  2.47 us (2%)
    pallas_call x1, Pallas kernels, run_experts(): pl.pallas_call(functools.partial(experts_kernel, width), out_shape=jax.Sh...  83.5 us
    pallas_call x1, Pallas kernels, run_front(): pl.pallas_call(functools.partial(front_kernel, chips), out_shape=[jax.Sha...  42.8 us
    unnamed x11, local copies, waits for them, and re-layouts  4.93 us
    reshape x4, local copies, waits for them, and re-layouts, run_front(): flat = [part.reshape(rows, -1) for part in lean + broad]  3.87 us

profile of v2, /device:TPU:0, one launch (start us, length us, event | category | flops | bytes accessed | tf_op | source)
XLA Modules:
  0.0 143.2 jit_solution(16312745106551254535)
XLA Ops:
  0.0 0.8 pad_maximum_fusion.lean_gain
  0.9 0.8 fusion.18
  1.6 0.7 fusion.9
  2.3 0.7 reduce-precision_subtract_fusion.1
  3.1 0.7 fusion.19
  3.8 0.2 fusion.1
  4.0 0.9 copy.26.lean_k
  4.9 1.0 copy.27.lean_v
  5.9 0.2 select_select_fusion.route_columns
  6.1 1.0 copy.25.lean_q
  7.1 1.0 copy.34
  8.1 1.0 copy_bitcast_fusion.1
  9.1 1.5 %sine_multiply_fusion = (f32[192,256]{1,0:T(8,128)S(1)}, f32[192,256]{1,0:T(8,128)S(1)}) fusion(f32[256]{0:T(256)} %constant.104, f32[256]{0:T(256)} %constant.103, f32[192]{0:T(256)S(1)} %get-tuple-element.20, f32[192]{0:T(256)S(1)} %get-tuple-element.21, pred[256]{0:T(512)(128)(4,1)} %constant.102), kind=kLoop, calls=%fused_computation.9 | loop fusion | flops 147456 | bytes 397056 | tf_op jit(solution)/shard_map/mul | solution.py:476
  10.5 0.0 copy-start.1
  10.6 1.0 copy-done.1
  11.5 0.0 copy-start.2
  11.5 0.7 copy-done.2
  12.3 0.7 copy-done.3
  12.9 0.7 copy-done.4
  13.6 42.8 %shard_map.199 = (f32[192,1024]{1,0:T(8,128)S(1)}, bf16[384,1152]{1,0:T(8,128)(2,1)S(1)}) custom-call(bf16[192,256]{1,0:T(8,128)(2,1)S(1)} %copy.25.lean_q, bf16[192,128]{1,0:T(8,128)(2,1)S(1)} %copy.26.lean_k, bf16[192,128]{1,0:T(8,128)(2,1)S(1)} %copy.27.lean_v, bf16[192,512]{1,0:T(8,128)(2,1)S(1)} %bitcast.28, ...), custom_call_target="tpu_custom_call" | custom-call | tf_op jit(solution)/shard_map/pallas_call | solution.py:441
  56.5 0.0 copy-start
  56.5 0.9 copy-done
  57.4 83.5 %shard_map.200 = bf16[4,96,1024]{2,1,0:T(8,128)(2,1)} custom-call(bf16[4,96,1152]{2,1,0:T(8,128)(2,1)} %bitcast.27, bf16[4,1024,512]{2,1,0:T(8,128)(2,1)} %bitcast.31, bf16[4,1024,512]{2,1,0:T(8,128)(2,1)} %bitcast.32, bf16[4,512,1024]{2,1,0:T(8,128)(2,1)} %bitcast.33), custom_call_target="tpu_custom_call" | custom-call | tf_op jit(solution)/shard_map/pallas_call | solution.py:681
  140.9 2.3 %fusion = bf16[192,1024]{1,0:T(8,128)(2,1)} fusion(f32[192,1024]{1,0:T(8,128)S(1)} %get-tuple-element.7, bf16[384,1024]{1,0:T(8,128)(2,1)} %bitcast.34, s32[192]{0:T(256)S(1)} %fusion.13), kind=kOutput, calls=%fused_computation.1 | convolution fusion | flops 151461888 | bytes 1966848 | tf_op jit(solution)/shard_map/dot_general | solution.py:775
  (10 shorter events, 0.1 us)
Async XLA Ops:
  10.5 1.0 copy-start.1
  11.5 0.7 copy-start.2
  12.3 0.7 copy-start.3
  12.9 0.7 copy-start.4
  56.5 0.9 copy-start

commit v3 on v2

--- a/solution.py
+++ b/solution.py
@@ -513,27 +513,26 @@
 ):
     z, core, tp, sibling, x_peer, y_peer, chunks = place()
     chips, cap = out_going.shape[0], out_going.shape[1]
-    ff = gate_acc.shape[1]
-    half = 2 * cap
+    part = cap // 2
     ahead = [{"sp": ((z + d) % chips) * 2 + core, "tp": tp} for d in range(chips)]
     behind = [{"sp": ((z + chips - d) % chips) * 2 + core, "tp": tp} for d in range(chips)]
     enter(ahead[1:] + [sibling, x_peer, y_peer])
 
     def slot(d, r, side=0):
-        return rows.at[d // 2, r, pl.ds(side * half + (d % 2) * cap, cap)]
-
-    Z, X, Y, RELAY, SIDE = 0, 1, 2, 3, 4
+        return rows.at[d, r, pl.ds(side * cap, cap)]
+
+    Z, X, Y, VIA_X, VIA_Y, SIDE = 0, 1, 2, 3, 4, 5
     pending = []
+    arrivals = {}
 
     def send(source, target, kind, d, device):
         copy = remote(source, target, send_sem.at[kind, d], recv_sem.at[kind, d], device)
         copy.start()
         pending.append(copy)
-        return copy
-
-    arrivals = {}
+        arrivals[kind, d] = copy
+
     for d in range(1, chips):
-        arrivals[Z, d] = send(out_going.at[d], slot(d, 0), Z, d, ahead[d])
+        send(out_going.at[d], slot(d, 0), Z, d, ahead[d])
     loads = [
         pltpu.make_async_copy(source, target, w_sem.at[i])
         for i, (source, target) in enumerate(
@@ -541,133 +540,124 @@
         )
     ]
 
+    def to_side(d, r):
+        source = out_going.at[0] if d == 0 and r == 0 else slot(d, r)
+        send(source, slot(d, r, 1), SIDE + r, d, sibling)
+
     def spread(d):
         source = out_going.at[0] if d == 0 else slot(d, 0)
         if d:
             arrivals[Z, d].wait_recv()
-        arrivals[X, d] = send(source, slot(d, 1), X, d, x_peer)
-        arrivals[Y, d] = send(source, slot(d, 2), Y, d, y_peer)
-        arrivals[SIDE, d] = send(source, slot(d, 0, 1), SIDE, d, sibling)
-
-    def to_side(d, r):
-        arrivals[SIDE + r, d] = send(slot(d, r), slot(d, r, 1), SIDE + r, d, sibling)
+        send(source, slot(d, 1), X, d, x_peer)
+        send(source, slot(d, 2), Y, d, y_peer)
+        to_side(d, 0)
 
     def relay(d):
-        arrivals[X, d].wait_recv()
-        if d % 2 == 0:
-            arrivals[RELAY, d] = send(slot(d, 1), slot(d, 3), RELAY, d, y_peer)
-        to_side(d, 1)
-        arrivals[Y, d].wait_recv()
-        if d % 2 == 1:
-            arrivals[RELAY, d] = send(slot(d, 2), slot(d, 3), RELAY, d, x_peer)
-        to_side(d, 2)
-
-    def project(p, r):
-        for d in (2 * p, 2 * p + 1):
+        for kind, r, peer in ((X, 1, y_peer), (Y, 2, x_peer)):
+            arrivals[kind, d].wait_recv()
+            piece = pl.ds((r - 1) * part, part)
+            send(rows.at[d, r, piece], rows.at[d, 3, piece], VIA_X + r - 1, d, peer)
+            to_side(d, r)
+
+    def project(d):
+        for r in range(4):
+            if r == 3:
+                arrivals[VIA_X, d].wait_recv()
+                arrivals[VIA_Y, d].wait_recv()
+                to_side(d, 3)
             arrivals[SIDE + r, d].wait_recv()
-        block = rows[p, r, :, pl.ds(0, width)]
-        for weight, total in ((gate_w, gate_acc), (up_w, up_acc)):
-            part = jnp.dot(block, weight[chunks[r]], preferred_element_type=jnp.float32)
-            if r == 0:
-                total[...] = part
-            else:
-                total[...] += part
-
-    def activate(p):
+            block = rows[d, r, :, pl.ds(0, width)]
+            for weight, total in ((gate_w, gate_acc), (up_w, up_acc)):
+                product = jnp.dot(block, weight[chunks[r]], preferred_element_type=jnp.float32)
+                if r == 0:
+                    total[...] = product
+                else:
+                    total[...] += product
         squares = 0.0
         for r in range(4):
-            extra = rows[p, r, :, pl.ds(width, EXTRA)].astype(jnp.float32)
+            extra = rows[d, r, :, pl.ds(width, EXTRA)].astype(jnp.float32)
             squares = squares + extra[:, 0:1] + extra[:, 1:2]
         scale = lax.rsqrt(squares / (4 * width) + epsilon)
         gate_value = gate_acc[...] * scale
         up_value = up_acc[...] * scale
-        hidden[p, 0] = (gate_value / (1.0 + jnp.exp(-gate_value)) * up_value).astype(jnp.bfloat16)
-        for k, peer in ((0, x_peer), (1, y_peer)):
-            copy = remote(
-                hidden.at[p, 0], hidden.at[p, 1 + k], h_send.at[p, k], h_recv.at[p, k], peer
-            )
-            copy.start()
-            pending.append(copy)
-            arrivals["h", p, k] = copy
-
-    def relay_hidden(p):
+        hidden[d, 0] = (gate_value / (1.0 + jnp.exp(-gate_value)) * up_value).astype(jnp.bfloat16)
+
+    def send_hidden_piece(d, k, source, target, peer):
+        copy = remote(source, target, h_send.at[d, k], h_recv.at[d, k], peer)
+        copy.start()
+        pending.append(copy)
+        arrivals["h", d, k] = copy
+
+    def spread_hidden(d):
+        send_hidden_piece(d, 0, hidden.at[d, 0], hidden.at[d, 1], x_peer)
+        send_hidden_piece(d, 1, hidden.at[d, 0], hidden.at[d, 2], y_peer)
+
+    def relay_hidden(d):
         for k, peer in ((0, y_peer), (1, x_peer)):
-            arrivals["h", p, k].wait_recv()
-            part = pl.ds(k * half, half)
-            copy = remote(
-                hidden.at[p, 1 + k, part],
-                hidden.at[p, 3, part],
-                h_send.at[p, 2 + k],
-                h_recv.at[p, 2 + k],
-                peer,
-            )
-            copy.start()
-            pending.append(copy)
-            arrivals["h", p, 2 + k] = copy
-
-    def last_slot(p):
-        for d in (2 * p, 2 * p + 1):
-            arrivals[RELAY, d].wait_recv()
-            to_side(d, 3)
-        project(p, 3)
-        activate(p)
-
-    def finish(p):
-        for r in range(3):
-            part = jnp.dot(hidden[p, r], down_w[chunks[r]], preferred_element_type=jnp.float32)
+            arrivals["h", d, k].wait_recv()
+            piece = pl.ds(k * cap, cap)
+            send_hidden_piece(d, 2 + k, hidden.at[d, 1 + k, piece], hidden.at[d, 3, piece], peer)
+
+    def finish(d):
+        for r in range(4):
+            if r == 3:
+                arrivals["h", d, 2].wait_recv()
+                arrivals["h", d, 3].wait_recv()
+            product = jnp.dot(hidden[d, r], down_w[chunks[r]], preferred_element_type=jnp.float32)
             if r == 0:
-                result[...] = part
+                result[...] = product
             else:
-                result[...] += part
-        for k in (2, 3):
-            arrivals["h", p, k].wait_recv()
-        result[...] += jnp.dot(hidden[p, 3], down_w[chunks[3]], preferred_element_type=jnp.float32)
-        extra = rows[p, 0, :, pl.ds(width, EXTRA)].astype(jnp.float32)
+                result[...] += product
+        extra = rows[d, 0, :, pl.ds(width, EXTRA)].astype(jnp.float32)
         low = extra[:, 2:3] + extra[:, 3:4]
         high = extra[:, 4:5] + extra[:, 5:6]
         share = low + (high - low) * core.astype(jnp.float32)
-        swap_send[p] = (result[half:, :] * share[half:]).astype(jnp.bfloat16)
-        copy = remote(swap_send.at[p], swap_recv.at[p], e_send.at[p], e_recv.at[p], sibling)
+        swap_send[d] = (result[cap:, :] * share[cap:]).astype(jnp.bfloat16)
+        copy = remote(swap_send.at[d], swap_recv.at[d], e_send.at[d], e_recv.at[d], sibling)
         copy.start()
         pending.append(copy)
-        kept = result[:half, :] * share[:half]
+        kept = result[:cap, :] * share[:cap]
         copy.wait_recv()
-        total = (kept + swap_recv[p].astype(jnp.float32)).astype(jnp.bfloat16)
-        back[p] = total
-        for d in (2 * p, 2 * p + 1):
-            part = pl.ds((d % 2) * cap, cap)
-            if d == 0:
-                out_ref[0] = total[:cap]
-                continue
-            copy = remote(back.at[p, part], out_ref.at[d], b_send.at[d], b_recv.at[d], behind[d])
-            copy.start()
-            pending.append(copy)
-            arrivals["b", d] = copy
+        total = (kept + swap_recv[d].astype(jnp.float32)).astype(jnp.bfloat16)
+        if d == 0:
+            out_ref[0] = total
+            return
+        back[d] = total
+        copy = remote(back.at[d], out_ref.at[d], b_send.at[d], b_recv.at[d], behind[d])
+        copy.start()
+        pending.append(copy)
+        arrivals["b", d] = copy
 
     spread(0)
     for copy in loads:
         copy.start()
     rows[0, 0, pl.ds(0, cap)] = out_going[0]
+    relay(0)
     spread(1)
-    relay(0)
     relay(1)
-    spread(2)
-    spread(3)
     loads[0].wait()
     loads[1].wait()
-    for r in range(3):
-        project(0, r)
-    last_slot(0)
+    project(0)
+    spread(2)
+    project(1)
+    spread_hidden(1)
     relay(2)
+    spread(3)
+    relay_hidden(1)
+    project(2)
+    spread_hidden(2)
     relay(3)
+    loads[2].wait()
+    finish(1)
+    spread_hidden(0)
+    relay_hidden(2)
+    project(3)
+    spread_hidden(3)
+    finish(2)
     relay_hidden(0)
-    for r in range(3):
-        project(1, r)
-    last_slot(1)
-    loads[2].wait()
+    relay_hidden(3)
+    finish(3)
     finish(0)
-    relay_hidden(1)
-    finish(1)
     for d in range(1, chips):
         arrivals["b", d].wait_recv()
     for copy in pending:
@@ -685,26 +675,26 @@
         + [pl.BlockSpec(memory_space=pl.ANY)] * 3,
         out_specs=pl.BlockSpec(memory_space=pltpu.VMEM),
         scratch_shapes=[
-            pltpu.VMEM((2, 4, 4 * cap, padded), jnp.bfloat16),
+            pltpu.VMEM((chips, 4, 2 * cap, padded), jnp.bfloat16),
             pltpu.VMEM((4, width, ff), jnp.bfloat16),
             pltpu.VMEM((4, width, ff), jnp.bfloat16),
             pltpu.VMEM((4, ff, features), jnp.bfloat16),
-            pltpu.VMEM((2, 4, 4 * cap, ff), jnp.bfloat16),
-            pltpu.VMEM((4 * cap, ff), jnp.float32),
-            pltpu.VMEM((4 * cap, ff), jnp.float32),
-            pltpu.VMEM((4 * cap, features), jnp.float32),
-            pltpu.VMEM((2, 2 * cap, features), jnp.bfloat16),
-            pltpu.VMEM((2, 2 * cap, features), jnp.bfloat16),
-            pltpu.VMEM((2, 2 * cap, features), jnp.bfloat16),
+            pltpu.VMEM((chips, 4, 2 * cap, ff), jnp.bfloat16),
+            pltpu.VMEM((2 * cap, ff), jnp.float32),
+            pltpu.VMEM((2 * cap, ff), jnp.float32),
+            pltpu.VMEM((2 * cap, features), jnp.float32),
+            pltpu.VMEM((chips, cap, features), jnp.bfloat16),
+            pltpu.VMEM((chips, cap, features), jnp.bfloat16),
+            pltpu.VMEM((chips, cap, features), jnp.bfloat16),
             pltpu.SemaphoreType.DMA((3,)),
-            pltpu.SemaphoreType.DMA((8, 4)),
-            pltpu.SemaphoreType.DMA((8, 4)),
-            pltpu.SemaphoreType.DMA((2, 4)),
-            pltpu.SemaphoreType.DMA((2, 4)),
-            pltpu.SemaphoreType.DMA((2,)),
-            pltpu.SemaphoreType.DMA((2,)),
-            pltpu.SemaphoreType.DMA((4,)),
-            pltpu.SemaphoreType.DMA((4,)),
+            pltpu.SemaphoreType.DMA((9, chips)),
+            pltpu.SemaphoreType.DMA((9, chips)),
+            pltpu.SemaphoreType.DMA((chips, 4)),
+            pltpu.SemaphoreType.DMA((chips, 4)),
+            pltpu.SemaphoreType.DMA((chips,)),
+            pltpu.SemaphoreType.DMA((chips,)),
+            pltpu.SemaphoreType.DMA((chips,)),
+            pltpu.SemaphoreType.DMA((chips,)),
         ],
         compiler_params=pltpu.CompilerParams(
             collective_id=2, has_side_effects=True, vmem_limit_bytes=56 * 1024 * 1024

time: 144 us -> 136 us (0.944)
  Pallas kernels: 126 us -> 117 us
    pallas_call x1, Pallas kernels: 83.5 us -> 74.2 us  [run_experts(): pl.pallas_call(functools.partial(experts_kernel, width), out_shape=jax.Sh...]
where the time goes in v3:
time: 136 us; the launch traced here: 134 us
  Pallas kernels  117 us (86%)
  local copies, waits for them, and re-layouts  8.8 us (6%)
  other arithmetic  5.46 us (4%)
  matrix products  2.47 us (2%)
    pallas_call x1, Pallas kernels, run_experts(): pl.pallas_call(functools.partial(experts_kernel, width), out_shape=jax.Sh...  74.2 us
    pallas_call x1, Pallas kernels, run_front(): pl.pallas_call(functools.partial(front_kernel, chips), out_shape=[jax.Sha...  43 us
    unnamed x11, local copies, waits for them, and re-layouts  4.93 us
    reshape x4, local copies, waits for them, and re-layouts, run_front(): flat = [part.reshape(rows, -1) for part in lean + broad]  3.87 us

profile of v3, /device:TPU:0, one launch (start us, length us, event | category | flops | bytes accessed | tf_op | source)
XLA Modules:
  0.0 134.1 jit_solution(4574666791166359729)
XLA Ops:
  0.0 0.8 pad_maximum_fusion.lean_gain
  0.9 0.8 fusion.18
  1.6 0.7 fusion.9
  2.3 0.7 reduce-precision_subtract_fusion.1
  3.1 0.7 fusion.19
  3.8 0.2 fusion.1
  4.0 0.9 copy.26.lean_k
  4.9 1.0 copy.27.lean_v
  5.9 0.2 select_select_fusion.route_columns
  6.1 1.0 copy.25.lean_q
  7.1 1.0 copy.34
  8.1 1.0 copy_bitcast_fusion.1
  9.1 1.5 %sine_multiply_fusion = (f32[192,256]{1,0:T(8,128)S(1)}, f32[192,256]{1,0:T(8,128)S(1)}) fusion(f32[256]{0:T(256)} %constant.104, f32[256]{0:T(256)} %constant.103, f32[192]{0:T(256)S(1)} %get-tuple-element.20, f32[192]{0:T(256)S(1)} %get-tuple-element.21, pred[256]{0:T(512)(128)(4,1)} %constant.102), kind=kLoop, calls=%fused_computation.9 | loop fusion | flops 147456 | bytes 397056 | tf_op jit(solution)/shard_map/mul | solution.py:476
  10.5 0.0 copy-start.1
  10.6 1.0 copy-done.1
  11.5 0.0 copy-start.2
  11.5 0.7 copy-done.2
  12.3 0.7 copy-done.3
  12.9 0.7 copy-done.4
  13.6 43.0 %shard_map.199 = (f32[192,1024]{1,0:T(8,128)S(1)}, bf16[384,1152]{1,0:T(8,128)(2,1)S(1)}) custom-call(bf16[192,256]{1,0:T(8,128)(2,1)S(1)} %copy.25.lean_q, bf16[192,128]{1,0:T(8,128)(2,1)S(1)} %copy.26.lean_k, bf16[192,128]{1,0:T(8,128)(2,1)S(1)} %copy.27.lean_v, bf16[192,512]{1,0:T(8,128)(2,1)S(1)} %bitcast.28, ...), custom_call_target="tpu_custom_call" | custom-call | tf_op jit(solution)/shard_map/pallas_call | solution.py:441
  56.6 0.0 copy-start
  56.7 0.9 copy-done
  57.6 74.2 %shard_map.200 = bf16[4,96,1024]{2,1,0:T(8,128)(2,1)} custom-call(bf16[4,96,1152]{2,1,0:T(8,128)(2,1)} %bitcast.27, bf16[4,1024,512]{2,1,0:T(8,128)(2,1)} %bitcast.31, bf16[4,1024,512]{2,1,0:T(8,128)(2,1)} %bitcast.32, bf16[4,512,1024]{2,1,0:T(8,128)(2,1)} %bitcast.33), custom_call_target="tpu_custom_call" | custom-call | tf_op jit(solution)/shard_map/pallas_call | solution.py:671
  131.8 2.3 %fusion = bf16[192,1024]{1,0:T(8,128)(2,1)} fusion(f32[192,1024]{1,0:T(8,128)S(1)} %get-tuple-element.7, bf16[384,1024]{1,0:T(8,128)(2,1)} %bitcast.34, s32[192]{0:T(256)S(1)} %fusion.13), kind=kOutput, calls=%fused_computation.1 | convolution fusion | flops 151461888 | bytes 1966848 | tf_op jit(solution)/shard_map/dot_general | solution.py:765
  (10 shorter events, 0.1 us)
Async XLA Ops:
  10.5 1.0 copy-start.1
  11.5 0.7 copy-start.2
  12.3 0.7 copy-start.3
  12.9 0.7 copy-start.4
  56.6 0.9 copy-start
